TPU v7x, 128 devices: a whole 4x4x4 slice. The times are simulated.
128 devices in a mesh: rep: 2 (over z_hi), fs: 32 (over z_lo, y, x), tp: 2 (over core).
Axes of the slice: x: 4, y: 4, z: 4 (z_hi: 2, z_lo: 2; z = z_hi * 2 + z_lo), core: 2. Of those that a mesh axis runs over, the one named last changes fastest.
Arguments:
- tokens: bfloat16 [65536, 2048], P(('rep', 'fs'), 'tp'), may hold values from -13 to 13
- norm_gains: float32 [4, 2048], replicated, may hold values from 0.1 to 1.9
- mix_weight: float32 [2048, 2048], P('fs', 'tp'), may hold values from -0.125 to 0.125
- mix_scale: float32 [32, 64], P('tp', 'fs'), may hold values from 0.5 to 2
- group_weight: float32 [4, 512, 512], P('tp', 'fs'), may hold values from -0.25 to 0.25
- group_scale: float32 [32, 64], P('tp', 'fs'), may hold values from 0.35 to 2.9
- up_weight: float32 [2048, 4096], P('fs', 'tp'), may hold values from -0.125 to 0.125
- up_scale: float32 [64, 64], P('tp', 'fs'), may hold values from 0.5 to 2
- down_weight: float32 [4096, 2048], P('tp', 'fs'), may hold values from -0.09375 to 0.09375
- down_scale: float32 [32, 64], P('tp', 'fs'), may hold values from 0.35 to 2.9
Outputs:
- layer_out: bfloat16 [65536, 2048], P(('rep', 'fs'), 'tp')
All inputs are finite; a program needn't handle non-finite values.
Results may differ from a plain program's by a relative error of at most 0.0083.
Values may be sent and summed in bfloat16 or wider, within the bound.
A program may use at most 128 MiB of HBM per device.

v0:
```python
import jax
import jax.numpy as jnp
from jax import lax
from jax.sharding import Mesh
from jax.sharding import PartitionSpec as P

FS = ("fs_0", "fs_1", "fs_2")
REP_FS = ("rep", "fs_0", "fs_1", "fs_2")


epsilon = 1e-06
widest = 16


def sent_to_all(x, axis):
    copies = jnp.broadcast_to(x, (lax.axis_size(axis), *x.shape))
    return lax.all_to_all(copies, axis, split_axis=0, concat_axis=0, tiled=True)


def taken_together(x, axis):
    everything = sent_to_all(x, axis)
    return jnp.sum(everything, axis=0)


def rows_first(arrays, axis, dims):
    turned = [jnp.moveaxis(a, dim, 0) for a, dim in zip(arrays, dims)]
    widths = [t[0].size for t in turned]
    both = jnp.concatenate([t.reshape(-1, w) for t, w in zip(turned, widths)], axis=1)
    out = lax.all_gather(both, axis, axis=0, tiled=True)
    pieces = jnp.split(out, [sum(widths[:k]) for k in range(1, len(widths))], axis=1)
    return tuple(
        (
            jnp.moveaxis(b.reshape(-1, *t.shape[1:]), 0, dim)
            for b, t, dim in zip(pieces, turned, dims)
        )
    )


def in_order(pieces, dim):
    shape = list(pieces.shape[1:])
    shape[dim] *= pieces.shape[0]
    return jnp.moveaxis(pieces, 0, dim).reshape(shape)


def gathered_copies(x, axis, dim):
    pieces = sent_to_all(x, axis)
    return in_order(pieces, dim)


def all_blocks(x, axes, order):
    pieces = x[None]
    for k in order:
        pieces = lax.all_gather(pieces, axes[k], axis=0, tiled=True)
    carried = [lax.axis_size(axes[k]) for k in reversed(order)]
    pieces = pieces.reshape(*carried, *x.shape)
    turned = sorted(range(len(order)), key=lambda place: order[len(order) - 1 - place])
    return pieces.transpose(*turned, *range(len(order), pieces.ndim)).reshape(-1, *x.shape)


def whole_of(x, axes, order, dim):
    return in_order(all_blocks(x, axes, order), dim)


def cut_along(x, dim, length):
    shape = x.shape
    pieces = x.reshape(*shape[:dim], length, shape[dim] // length, *shape[dim + 1 :])
    return jnp.moveaxis(pieces, dim, 0)


def sum_at_owner(x, axis, dim):
    pieces = cut_along(x, dim, lax.axis_size(axis))
    arrived = lax.all_to_all(pieces, axis, split_axis=0, concat_axis=0, tiled=True)
    return arrived.astype(jnp.float32).sum(axis=0)


def rounded(values):
    return lax.optimization_barrier(values.astype(jnp.bfloat16)).astype(jnp.float32)


def pre_norm(part, gain):
    rows = lax.all_gather(part, "tp", axis=1, tiled=True).astype(jnp.float32)
    inverse = lax.rsqrt(jnp.mean(rows * rows, axis=1, keepdims=True) + epsilon)
    return (rows * inverse * gain).astype(jnp.bfloat16)


def post_norm(branch, gain, width):
    square_sum = taken_together(jnp.sum(branch * branch, axis=1), "tp")
    inverse = lax.rsqrt(square_sum / width + epsilon)
    return rounded(branch * inverse[:, None] * gain)


def fold_rows(left, piece):
    return jnp.dot(left, piece, preferred_element_type=jnp.float32)


def fold_groups(left, piece):
    return jnp.einsum("sgc,gcd->sgd", left, piece, preferred_element_type=jnp.float32)


def pool_local(mixed, first_group, group_count):
    length = mixed.shape[0]
    upward = mixed.astype(jnp.float32).reshape(length, group_count, -1)
    sums = jnp.concatenate(
        [jnp.zeros((widest + 1,) + upward.shape[1:], jnp.float32), jnp.cumsum(upward, axis=0)],
        axis=0,
    )
    position = jnp.arange(length, dtype=jnp.int32)
    pieces = []
    for local in range(group_count):
        window = jnp.left_shift(jnp.int32(2), first_group + local)
        upper = sums[widest + 1 :, local]
        lower = lax.dynamic_slice_in_dim(sums[:, local], widest + 1 - window, length, 0)
        count = jnp.minimum(position + 1, window).astype(jnp.float32)[:, None]
        pieces.append((upper - lower) / count - upward[:, local])
    return jnp.stack(pieces, axis=1).astype(jnp.bfloat16)


def on_device(
    tokens,
    norm_gains,
    mix_weight,
    mix_scale,
    group_weight,
    group_scale,
    up_weight,
    up_scale,
    down_weight,
    down_scale,
):
    length, half_width = tokens.shape
    width = half_width * lax.axis_size("tp")
    offset = lax.axis_index("tp") * half_width

    def own_gain(which):
        return lax.dynamic_slice_in_dim(norm_gains[which], offset, half_width)

    gathered = rows_first((mix_scale, group_scale, up_scale, down_scale), FS, (1, 1, 1, 1))
    mix_cols = gathered[0]
    normed = pre_norm(tokens, norm_gains[0])
    mixed = fold_rows(
        normed, lax.all_gather(mix_weight.astype(jnp.bfloat16), FS, axis=0, tiled=True)
    )
    mixed = (mixed * mix_cols.reshape(-1)).astype(jnp.bfloat16)
    group_count = group_weight.shape[0]
    pooled = pool_local(mixed, lax.axis_index("tp") * group_count, group_count)
    grouped = fold_groups(pooled, gathered_copies(group_weight.astype(jnp.bfloat16), FS, 1))
    group_cols = gathered[1]
    branch = rounded(grouped.reshape(length, half_width) * group_cols.reshape(-1))
    middle = (tokens.astype(jnp.float32) + post_norm(branch, own_gain(1), width)).astype(
        jnp.bfloat16
    )
    down_whole = lax.all_gather(down_weight.astype(jnp.bfloat16), FS, axis=1, tiled=True)
    normed_mid = pre_norm(middle, norm_gains[2])
    upward = fold_rows(normed_mid, whole_of(up_weight.astype(jnp.bfloat16), FS, (0, 1, 2), 0))
    up_cols = gathered[2]
    active = jnp.maximum(upward * up_cols.reshape(-1), 0.0)
    hidden = (active * active).astype(jnp.bfloat16)
    partial_sums = jnp.dot(hidden, down_whole, preferred_element_type=jnp.float32)
    total = sum_at_owner(partial_sums.astype(jnp.bfloat16), "tp", 1)
    down_cols = gathered[3]
    down = rounded(total * down_cols.reshape(-1))
    return (middle.astype(jnp.float32) + post_norm(down, own_gain(3), width)).astype(jnp.bfloat16)


def solution(mesh):
    finer = Mesh(
        mesh.devices.reshape(mesh.shape["rep"], 2, 4, 4, mesh.shape["tp"]),
        ("rep", "fs_0", "fs_1", "fs_2", "tp"),
    )
    in_specs = (
        P(REP_FS, "tp"),
        P(),
        P(FS, "tp"),
        P("tp", FS),
        P("tp", FS, None),
        P("tp", FS),
        P(FS, "tp"),
        P("tp", FS),
        P("tp", FS),
        P("tp", FS),
    )
    out_specs = P(REP_FS, "tp")
    return jax.shard_map(
        on_device, mesh=finer, in_specs=in_specs, out_specs=out_specs, check_vma=False
    )
```

profile of v0, /device:TPU:1, one launch (start us, length us, event | category | flops | bytes accessed | tf_op | source)
XLA Modules:
  0.0 560.3 jit_solution(2007830422461045758)
XLA Ops:
  10.9 9.2 %all-to-all-start = ((bf16[32,2,16,512]{3,2,1,0:T(8,128)(2,1)}), bf16[32,2,16,512]{3,2,1,0:T(8,128)(2,1)S(1)}, u32[]{:S(2)}, u32[]{:S(2)}) async-start(bf16[32,2,16,512]{3,2,1,0:T(8,128)(2,1)} %broadcast_in_dim.8), calls=%async_computation | async-start | bytes 2097152 | tf_op jit(solution)/shard_map/all_to_all | solution.py:17
  20.2 19.2 %all-gather = bf16[128,2048]{1,0:T(8,128)(2,1)} all-gather(bf16[64,2048]{1,0:T(8,128)(2,1)S(1)} %convert_element_type.104), channel_id=2, replica_groups=mesh['rep'=2,'fs_0'=2,'fs_1'=4,'fs_2'=4,'tp'=2] {'fs_0'}, dimensions={0}, use_global_device_ids=true | all-gather | bytes 786432 | tf_op jit(solution)/shard_map/all_gather | solution.py:53
  39.6 68.3 %all-gather.1 = f32[32,2,80]{2,1,0:T(2,128)S(1)} all-gather(f32[1,2,80]{2,1,0:T(2,128)S(1)} %maximum_bitcast_fusion), channel_id=1, replica_groups=mesh['rep'=2,'fs_0'=2,'fs_1'=4,'fs_2'=4,'tp'=2] {'fs_0','fs_1','fs_2'}, dimensions={0}, use_global_device_ids=true | all-gather | bytes 21120 | tf_op jit(solution)/shard_map/all_gather | solution.py:29
  108.4 3.1 fusion
  111.5 56.5 %all-gather.11.cloned.1.call-done = bf16[2048,1024]{1,0:T(8,128)(2,1)} async-done(((bf16[64,1024]{1,0:T(8,128)(2,1)}), bf16[2048,1024]{1,0:T(8,128)(2,1)}) %all-gather.11.cloned.1.call-update) | async-done | bytes 4194320 | tf_op jit(solution)/shard_map/all_gather | solution.py:141
  168.1 8.4 %multiply_convert_fusion.3 = bf16[1024,1024]{0,1:T(8,128)(2,1)S(1)} fusion(f32[1024]{0:T(1024)S(1)} %mul.139, bf16[2048,1024]{1,0:T(8,128)(2,1)} %all-gather.11.cloned.1.call-done, bf16[1024,2048]{1,0:T(8,128)(2,1)} %all-gather.9.cloned.1.call-done, f32[2048]{0:T(1024)S(1)} %bitcast.67, f32[1024]{0:T(1024)S(1)} %add_rsqrt_fusion.3), kind=kOutput, calls=%fused_computation.35 | convolution fusion | flops 4305453056 | bytes 10502144 | tf_op jit(solution)/shard_map/dot_general | solution.py:93
  176.5 3.2 copy.68
  179.7 4.6 fusion.17
  186.3 2.7 broadcast_add_fusion
  189.0 2.4 copy.70
  194.7 3.2 fusion.34
  198.0 5.6 copy.76
  203.5 2.8 multiply_convert_fusion.2
  206.8 24.1 %all_to_all.22 = f32[2,1,1024]{2,1,0:T(1,128)S(1)} all-to-all(f32[2,1,1024]{2,1,0:T(1,128)S(1)} %broadcast_in_dim.9), channel_id=1, replica_groups=mesh['rep'=2,'fs_0'=2,'fs_1'=4,'fs_2'=4,'tp'=2] {'tp'}, dimensions={0} | all-to-all | bytes 16384 | tf_op jit(solution)/shard_map/all_to_all | solution.py:17
  232.5 2.3 add_convert_fusion.1
  236.8 15.1 %all-gather.13.cloned.1.call-done = bf16[1024,2048]{1,0:T(8,128)(2,1)} async-done(((bf16[1024,1024]{1,0:T(8,128)(2,1)}), bf16[1024,2048]{1,0:T(8,128)(2,1)}) %all-gather.13.cloned.1.call-update) | async-done | bytes 4194320 | tf_op jit(solution)/shard_map/all_gather | solution.py:81
  251.8 3.1 fusion.3
  254.9 82.2 %all-gather.17.cloned.1.call-done = bf16[32,64,2048]{2,1,0:T(8,128)(2,1)} async-done(((bf16[8,64,2048]{2,1,0:T(8,128)(2,1)}), bf16[32,64,2048]{2,1,0:T(8,128)(2,1)}) %all-gather.17.cloned.1.call-update) | async-done | bytes 8388624 | tf_op jit(solution)/shard_map/all_gather | solution.py:53
  337.2 8.3 %copy.78 = bf16[2,4,4,64,2048]{4,3,2,1,0:T(8,128)(2,1)} copy(bf16[2,4,4,64,2048]{4,3,0,1,2:T(8,128)(2,1)} %bitcast.52) | data formatting | bytes 16777216 | tf_op jit(solution)/shard_map/transpose | solution.py:57
  345.5 140.3 %all-gather.19.cloned.1.call-done = bf16[2048,2048]{0,1:T(8,128)(2,1)} async-done(((bf16[2048,64]{0,1:T(8,128)(2,1)}), bf16[2048,2048]{0,1:T(8,128)(2,1)}) %all-gather.19.cloned.1.call-update) | async-done | bytes 8388624 | tf_op jit(solution)/shard_map/all_gather | solution.py:152
  485.7 25.6 %fusion.27 = bf16[1024,2048]{1,0:T(8,128)(2,1)} fusion(bf16[2048,2048]{0,1:T(8,128)(2,1)} %all-gather.19.cloned.1.call-done, bf16[2048,2048]{1,0:T(8,128)(2,1)} %bitcast.53, bf16[1024,2048]{1,0:T(8,128)(2,1)} %all-gather.13.cloned.1.call-done, f32[2048]{0:T(1024)S(1)} %mul.159, f32[2048]{0:T(1024)S(1)} %bitcast.66, f32[1024]{0:T(1024)S(1)} %add_rsqrt_fusion.1), kind=kOutput, calls=%fused_computation.40 | convolution fusion | flops 17198743552 | bytes 25186304 | tf_op jit(solution)/shard_map/dot_general | solution.py:158
  511.3 2.6 copy.94
  514.0 27.7 %all_to_all.23 = bf16[2,1024,1024]{2,1,0:T(8,128)(2,1)S(1)} all-to-all(bf16[2,1024,1024]{2,1,0:T(8,128)(2,1)S(1)} %bitcast.51), channel_id=1, replica_groups=mesh['rep'=2,'fs_0'=2,'fs_1'=4,'fs_2'=4,'tp'=2] {'tp'}, dimensions={0} | all-to-all | bytes 8388608 | tf_op jit(solution)/shard_map/all_to_all | solution.py:72
  545.2 3.9 all_to_all.24
  (80 shorter events, 22.3 us)
Async XLA Ops:
  6.5 13.7 %copy-start.5 = (f32[64,2048]{1,0:T(8,128)S(1)}, f32[64,2048]{1,0:T(8,128)}, u32[]{:S(2)}) copy-start(f32[64,2048]{1,0:T(8,128)} %param.16) | copy-start | bytes 1572868
  6.5 33.0 %copy-start.11 = (f32[16,2]{0,1:T(2,128)S(1)}, f32[16,2]{0,1:T(2,128)}, u32[]{:S(2)}) copy-start(f32[16,2]{0,1:T(2,128)} %param.13) | copy-start | bytes 388
  6.5 33.0 %copy-start.10 = (f32[16,2]{0,1:T(2,128)S(1)}, f32[16,2]{0,1:T(2,128)}, u32[]{:S(2)}) copy-start(f32[16,2]{0,1:T(2,128)} %param.15) | copy-start | bytes 388
  6.5 33.0 %copy-start.9 = (f32[32,2]{0,1:T(2,128)S(1)}, f32[32,2]{0,1:T(2,128)}, u32[]{:S(2)}) copy-start(f32[32,2]{0,1:T(2,128)} %param.17) | copy-start | bytes 772
  6.5 33.0 %copy-start.8 = (f32[16,2]{0,1:T(2,128)S(1)}, f32[16,2]{0,1:T(2,128)}, u32[]{:S(2)}) copy-start(f32[16,2]{0,1:T(2,128)} %param.19) | copy-start | bytes 388
  6.5 101.7 %copy-start.7 = (f32[4,2048]{1,0:T(4,128)S(1)}, f32[4,2048]{1,0:T(4,128)}, u32[]{:S(2)}) copy-start(f32[4,2048]{1,0:T(4,128)} %param.11) | copy-start | bytes 98308
  6.6 101.9 %all-gather.9.cloned.1.call-start = ((), (), s32[]{:S(2)}) async-start(), calls=%async_computation.4 | async-start | bytes 6291456 | tf_op jit(solution)/shard_map/all_gather | solution.py:81
  7.3 160.8 %all-gather.11.cloned.1.call-start = ((), (), s32[]{:S(2)}) async-start(), calls=%async_computation.5 | async-start | bytes 4325376 | tf_op jit(solution)/shard_map/all_gather | solution.py:141
  10.9 97.4 %all-to-all-start = ((bf16[32,2,16,512]{3,2,1,0:T(8,128)(2,1)}), bf16[32,2,16,512]{3,2,1,0:T(8,128)(2,1)S(1)}, u32[]{:S(2)}, u32[]{:S(2)}) async-start(bf16[32,2,16,512]{3,2,1,0:T(8,128)(2,1)} %broadcast_in_dim.8), calls=%async_computation | async-start | bytes 2097152 | tf_op jit(solution)/shard_map/all_to_all | solution.py:17
  20.1 214.7 %all-gather.15.cloned.1.call-start = ((), (), s32[]{:S(2)}) async-start(), calls=%async_computation.7 | async-start | bytes 2621440 | tf_op jit(solution)/shard_map/all_gather | solution.py:53
  39.4 212.4 %all-gather.13.cloned.1.call-start = ((), (), s32[]{:S(2)}) async-start(), calls=%async_computation.6 | async-start | bytes 6291456 | tf_op jit(solution)/shard_map/all_gather | solution.py:81
  184.3 2.0 copy-start.3
  191.5 2.2 copy-start
  230.9 1.6 copy-start.4
  232.5 3.2 copy-start.6
  234.8 102.4 %all-gather.17.cloned.1.call-start = ((), (), s32[]{:S(2)}) async-start(), calls=%async_computation.8 | async-start | bytes 10485760 | tf_op jit(solution)/shard_map/all_gather | solution.py:53
  235.4 250.3 %all-gather.19.cloned.1.call-start = ((), (), s32[]{:S(2)}) async-start(), calls=%async_computation.9 | async-start | bytes 8650752 | tf_op jit(solution)/shard_map/all_gather | solution.py:152
  543.3 1.3 copy-start.2
  544.7 6.5 %copy-start.1 = (bf16[1024,1024]{1,0:T(8,128)(2,1)S(1)}, bf16[1024,1024]{1,0:T(8,128)(2,1)}, u32[]{:S(2)}) copy-start(bf16[1024,1024]{1,0:T(8,128)(2,1)} %add_convert_fusion.1) | copy-start | bytes 6291460
Sparse Core Ops, SparseCore 0:
  9.0 19.9 all-gather.8
  30.7 137.3 all-gather.10
  169.8 50.8 all-gather.14
  234.9 16.8 all-gather.12
  253.4 83.7 all-gather.16
  338.7 147.0 all-gather.18
where the time goes:
time: 561 us; the launch traced here: 560 us
  waiting for transfers between devices  295 us (53%)
  blocking collectives  143 us (25%)
  matrix products  37.3 us (7%)
  local copies, waits for them, and re-layouts  30.6 us (5%)
  other arithmetic  30.6 us (5%)
  between operations  13.8 us (2%)
  starting transfers between devices  9.67 us (2%)
    all_gather x1, waiting for transfers between devices, on_device(): lax.all_gather(down_weight.astype(jnp.bfloat16), FS, axis=1, tiled=True)  140 us
    all_gather x2, waiting for transfers between devices, all_blocks(): pieces = lax.all_gather(pieces, axes[k], axis=0, tiled=True)  82.3 us
    all_gather x1, blocking collectives, rows_first(): out = lax.all_gather(both, axis, axis=0, tiled=True)  68.3 us
    all_gather x1, waiting for transfers between devices, on_device(): lax.all_gather(mix_weight.astype(jnp.bfloat16), FS, axis=0, tiled=True)  56.5 us
    all_to_all x2, blocking collectives, sent_to_all(): return lax.all_to_all(copies, axis, split_axis=0, concat_axis=0, tiled=True)  27.9 us
    all_to_all x1, blocking collectives, sum_at_owner(): lax.all_to_all(pieces, axis, split_axis=0, concat_axis=0, tiled=True)  27.7 us
    dot_general x1, matrix products, on_device(): jnp.dot(hidden, down_whole, preferred_element_type=jnp.float32)  25.6 us
    all_gather x1, blocking collectives, all_blocks(): pieces = lax.all_gather(pieces, axes[k], axis=0, tiled=True)  19.2 us
  transfers between devices with their start and end apart: 7, of which 4 were waited for; matrix products, arithmetic and copies ran while one was open for 10% of the time, Pallas kernels for 0%

commit v1 on v0

v1 whole, which is shorter than its diff:
```python
import functools

import jax
import jax.numpy as jnp
from jax import lax
from jax.experimental import pallas as pl
from jax.experimental.pallas import tpu as pltpu
from jax.sharding import Mesh
from jax.sharding import PartitionSpec as P

FS = ("fs_0", "fs_1", "fs_2")
REP_FS = ("rep", "fs_0", "fs_1", "fs_2")
MESH = pl.DeviceIdType.MESH
ORDERS = ("xyz", "yxz", "xzy", "yzx")
ALL = slice(None)
EPS = 1e-06

LENGTH = 1024
HALF = 1024
GW = 512
NB = 5
ROWS = (80, 64, 64, 64, 64)
BLOCK = 256
NR = LENGTH // BLOCK
F32, BF16 = jnp.float32, jnp.bfloat16


def dot(a, b):
    return jnp.dot(a, b, preferred_element_type=F32)


def dot_t(a, b):
    return lax.dot_general(a, b, (((1,), (1,)), ((), ())), preferred_element_type=F32)


def spot():
    return dict(
        z=lax.axis_index("rep") * 2 + lax.axis_index("fs_0"),
        y=lax.axis_index("fs_1"),
        x=lax.axis_index("fs_2"),
        t=lax.axis_index("tp"),
    )


def to(axis, at):
    if axis == "x":
        return {"fs_2": at}
    if axis == "y":
        return {"fs_1": at}
    if axis == "z":
        return {"rep": at // 2, "fs_0": at % 2}
    return {"tp": at}


def send(src, dst, send_sem, recv_sem, axis, at):
    return pltpu.make_async_remote_copy(
        src_ref=src,
        dst_ref=dst,
        send_sem=send_sem,
        recv_sem=recv_sem,
        device_id=to(axis, at),
        device_id_type=MESH,
    )


class Gather:
    def __init__(self, bufs, send_sem, recv_sem, me):
        self.bufs, self.send_sem, self.recv_sem, self.me = bufs, send_sem, recv_sem, me
        self.sent = []
        self.steps = {
            (b, c): self.plan(b, c, order)
            for b in range(len(bufs))
            for c, order in enumerate(ORDERS)
        }

    def region(self, b, c, at, half):
        lane = 256 * c + (128 * half if half is not None else 0)
        width = 256 if half is None else 128
        return self.bufs[b].at[at["z"], at["y"], at["x"], :, pl.ds(lane, width)]

    def copy(self, b, c, slot, ref, axis, at):
        return send(
            ref, ref, self.send_sem.at[b, c, slot], self.recv_sem.at[b, c, slot], axis, at
        )

    def plan(self, b, c, order):
        me = self.me
        own = dict(z=me["z"] % 2, y=me["y"], x=me["x"])
        steps, slot = [], 0
        for axis in order:
            up, down, far = (lax.rem(me[axis] + d, 4) for d in (1, 3, 2))

            def part(i, half=None, own=own, axis=axis):
                return self.region(b, c, {**own, axis: i}, half)

            if axis == "z":
                here, other = own["z"], 1 - own["z"]
                steps.append(
                    (
                        [(slot, part(here, 0), axis, up), (slot + 1, part(here, 1), axis, down)],
                        [(slot, part(other, 0)), (slot + 1, part(other, 1))],
                    )
                )
                slot += 2
            else:
                here = me[axis]
                steps.append(
                    (
                        [(slot, part(here), axis, up), (slot + 1, part(here), axis, down)],
                        [(slot, part(down)), (slot + 1, part(up))],
                    )
                )
                steps.append(
                    (
                        [
                            (slot + 2, part(down, 0), axis, up),
                            (slot + 3, part(up, 1), axis, down),
                        ],
                        [(slot + 2, part(far, 0)), (slot + 3, part(far, 1))],
                    )
                )
                slot += 4
            own = {**own, axis: ALL}
        return steps

    def tick(self, b, s, colours=range(4)):
        for c in colours:
            if s > 0:
                for slot, ref in self.steps[b, c][s - 1][1]:
                    self.copy(b, c, slot, ref, "x", self.me["x"]).wait_recv()
            if s < 5:
                for slot, ref, axis, at in self.steps[b, c][s][0]:
                    copy = self.copy(b, c, slot, ref, axis, at)
                    copy.start()
                    self.sent.append(copy)

    def finish(self):
        for copy in self.sent:
            copy.wait_send()


def greet(me):
    barrier = pltpu.get_barrier_semaphore()
    peers = [("x", 1), ("x", 2), ("x", 3), ("y", 1), ("y", 2), ("y", 3), ("z", 1), ("z", 3)]
    for axis, d in peers:
        pl.semaphore_signal(
            barrier, inc=1, device_id=to(axis, lax.rem(me[axis] + d, 4)), device_id_type=MESH
        )
    pl.semaphore_signal(barrier, inc=1, device_id=to("t", 1 - me["t"]), device_id_type=MESH)
    pl.semaphore_wait(barrier, len(peers) + 1)


def kernel(
    tokens,
    gains,
    mix_w,
    group_w,
    up_w,
    down_w,
    tile,
    out,
    w0,
    w1,
    w2,
    w3,
    w4,
    x_buf,
    normed,
    mixed,
    branch,
    hidden,
    acc,
    part_out,
    part_in,
    squares,
    band,
    sc_in,
    sc_sum,
    scale,
    g_send,
    g_recv,
    load_sem,
    p_send,
    p_recv,
    s_send,
    s_recv,
):
    me = spot()
    t, other = me["t"], 1 - me["t"]
    here = (me["z"] % 2, me["y"], me["x"])
    bufs = (w0, w1, w2, w3, w4)
    gather = Gather(bufs, g_send, g_recv, me)
    sent = []

    def rows_of(i, size=BLOCK):
        return pl.ds(i * size, size)

    loads = []
    for i in range(NR):
        load = pltpu.make_async_copy(
            tokens.at[rows_of(i)], x_buf.at[t, rows_of(i)], load_sem.at[i]
        )
        load.start()
        loads.append(load)
    w0[here[0], here[1], here[2], 0:64] = mix_w[...].astype(BF16)
    w0[here[0], here[1], here[2], 64:80, 0:GW] = group_w[0].astype(BF16)
    w0[here[0], here[1], here[2], 64:80, GW:] = group_w[1].astype(BF16)
    greet(me)

    def share(kind, i, src, dst):
        copy = send(src, dst, p_send.at[kind, i], p_recv.at[kind, i], "t", other)
        copy.start()
        sent.append(copy)

    def arrived(kind, i, ref):
        send(ref, ref, p_send.at[kind, i], p_recv.at[kind, i], "t", other).wait_recv()

    gather.tick(0, 0)
    for i in range(NR):
        share(0, i, tokens.at[rows_of(i)], x_buf.at[t, rows_of(i)])

    def scale_send(slot, src, axis, at):
        copy = send(src, sc_in.at[slot], s_send.at[slot], s_recv.at[slot], axis, at)
        copy.start()
        sent.append(copy)

    def scale_wait(slot):
        send(sc_in.at[slot], sc_in.at[slot], s_send.at[slot], s_recv.at[slot], "t", other).wait_recv()

    def scales(step):
        if step == 0:
            for d in (1, 2, 3):
                scale_send(d - 1, tile, "x", lax.rem(me["x"] + d, 4))
        if step == 1:
            for d in (1, 2, 3):
                scale_wait(d - 1)
            sc_sum[0] = tile[...] + sc_in[0] + sc_in[1] + sc_in[2]
        if step == 2:
            for d in (1, 2, 3):
                scale_send(d + 2, sc_sum.at[0], "y", lax.rem(me["y"] + d, 4))
        if step == 3:
            for d in (1, 2, 3):
                scale_wait(d + 2)
            sc_sum[1] = sc_sum[0] + sc_in[3] + sc_in[4] + sc_in[5]
        if step == 4:
            scale_send(6, sc_sum.at[1], "z", me["z"] + 1 - 2 * (me["z"] % 2))
        if step == 5:
            scale_wait(6)
            whole = sc_sum[1] + sc_in[6]
            for q in range(40):
                scale[q // 8 : q // 8 + 1, 128 * (q % 8) : 128 * (q % 8) + 128] = whole[q : q + 1]

    def fill():
        up = up_w[...].astype(BF16)
        w1[here[0], here[1], here[2]] = up[:, 0:1024]
        w2[here[0], here[1], here[2]] = up[:, 1024:]
        eye = (
            lax.broadcasted_iota(jnp.int32, (64, 64), 0)
            == lax.broadcasted_iota(jnp.int32, (64, 64), 1)
        ).astype(BF16)
        turned = dot_t(eye, down_w[...].astype(BF16)).astype(BF16)
        w3[here[0], here[1], here[2]] = turned[:, 0:1024]
        w4[here[0], here[1], here[2]] = turned[:, 1024:]

    def bands():
        i = lax.broadcasted_iota(jnp.int32, (BLOCK, 2 * BLOCK), 0)
        j = lax.broadcasted_iota(jnp.int32, (BLOCK, 2 * BLOCK), 1) - BLOCK
        for g, window in enumerate((2 + 6 * t, 4 + 12 * t)):
            band[g] = jnp.where((j <= i) & (j > i - window), 1.0, 0.0).astype(BF16)

    def mean_inverse(total):
        return lax.rsqrt(total * (1.0 / (2 * HALF)) + EPS)

    def row_sum(v):
        return jnp.sum(v, axis=1, keepdims=True)

    SUB = 16

    def first_norm(i):
        loads[i].wait()
        arrived(0, i, x_buf.at[other, rows_of(i)])
        g0, g1 = gains[0:1, 0:HALF], gains[0:1, HALF:]

        def body(k, _):
            rows = pl.ds(pl.multiple_of(i * BLOCK + k * SUB, SUB), SUB)
            a, b = x_buf[0, rows].astype(F32), x_buf[1, rows].astype(F32)
            inverse = mean_inverse(row_sum(a * a + b * b))
            normed[rows, 0:HALF] = (a * inverse * g0).astype(BF16)
            normed[rows, HALF:] = (b * inverse * g1).astype(BF16)
            return 0

        lax.fori_loop(0, BLOCK // SUB, body, 0, unroll=2)

    def mix(c):
        cols = slice(256 * c, 256 * c + 256)
        weight = w0[:, :, :, 0:64, cols].reshape(2 * HALF, 256)

        def body(i, _):
            rows = pl.ds(pl.multiple_of(i * 512, 512), 512)
            mixed[rows, cols] = (dot(normed[rows], weight) * scale[0:1, cols]).astype(BF16)
            return 0

        lax.fori_loop(0, 2, body, 0)

    def pool(i):
        rows = slice(i * BLOCK, i * BLOCK + BLOCK)
        for g in range(2):
            cols = slice(GW * g, GW * g + GW)
            window = (2 + 6 * t, 4 + 12 * t)[g]
            own = mixed[rows, cols]
            if i == 0:
                sums = dot(band[g, :, BLOCK:], own)
                position = lax.broadcasted_iota(jnp.int32, (BLOCK, 1), 0)
                sums = sums / jnp.minimum(position + 1, window).astype(F32)
            else:
                sums = dot(band[g], mixed[rows.start - BLOCK : rows.stop, cols])
                sums = sums * (1.0 / jnp.full((BLOCK, 1), window, jnp.int32).astype(F32))
            pooled = (sums - own.astype(F32)).astype(BF16)
            weight = w0[:, :, :, 64:80, cols].reshape(GW, GW)
            branch[t, rows, cols] = (dot(pooled, weight) * scale[1:2, cols]).astype(BF16)

    def branch_share(i):
        share(1, i, branch.at[t, rows_of(i)], branch.at[t, rows_of(i)])

    def middle(i):
        arrived(1, i, branch.at[other, rows_of(i)])
        post = [gains[1:2, 0:HALF], gains[1:2, HALF:]]
        pre = [gains[2:3, 0:HALF], gains[2:3, HALF:]]

        def body(k, _):
            rows = pl.ds(pl.multiple_of(i * BLOCK + k * SUB, SUB), SUB)
            parts = [branch[h, rows].astype(F32) for h in range(2)]
            inverse = mean_inverse(row_sum(parts[0] * parts[0] + parts[1] * parts[1]))
            mids = []
            for h in range(2):
                add = (parts[h] * inverse * post[h]).astype(BF16).astype(F32)
                mid = (x_buf[h, rows].astype(F32) + add).astype(BF16)
                x_buf[h, rows] = mid
                mids.append(mid.astype(F32))
            inverse = mean_inverse(row_sum(mids[0] * mids[0] + mids[1] * mids[1]))
            for h in range(2):
                normed[rows, h * HALF : h * HALF + HALF] = (mids[h] * inverse * pre[h]).astype(BF16)
            return 0

        lax.fori_loop(0, BLOCK // SUB, body, 0, unroll=2)

    def up(b, c):
        cols = slice(256 * c, 256 * c + 256)
        place = slice((b - 1) * 1024 + 256 * c, (b - 1) * 1024 + 256 * c + 256)
        weight = bufs[b][:, :, :, :, cols].reshape(2 * HALF, 256)

        def body(i, _):
            rows = pl.ds(pl.multiple_of(i * 512, 512), 512)
            act = jnp.maximum(dot(normed[rows], weight) * scale[b + 1 : b + 2, cols], 0.0)
            hidden[rows, place] = (act * act).astype(BF16)
            return 0

        lax.fori_loop(0, 2, body, 0)

    def down_first(i):
        rows = pl.ds(i * 512, 512)
        left = hidden[rows, 0:1024]

        def body(k, _):
            weight = w3[k // 4, k % 4].reshape(256, 1024)
            acc[k // 4, rows, pl.ds(pl.multiple_of(k % 4 * 256, 256), 256)] = dot_t(left, weight)
            return 0

        lax.fori_loop(0, 8, body, 0)

    def down_second(i, half, target):
        rows = pl.ds(i * BLOCK, BLOCK)
        left = hidden[rows, 1024:]

        def body(k, _):
            weight = w4[half, k].reshape(256, 1024)
            cols = pl.ds(pl.multiple_of(k * 256, 256), 256)
            target[rows, cols] = (acc[half, rows, cols] + dot_t(left, weight)).astype(BF16)
            return 0

        lax.fori_loop(0, 4, body, 0)

    def part_share(i):
        share(2, i, part_out.at[rows_of(i)], part_in.at[rows_of(i)])

    def total(i):
        arrived(2, i, part_in.at[rows_of(i)])

        def body(k, _):
            rows = pl.ds(pl.multiple_of(i * BLOCK + k * SUB, SUB), SUB)
            both = mixed[rows].astype(F32) + part_in[rows].astype(F32)
            down = (both * scale[4:5]).astype(BF16)
            mixed[rows] = down
            down = down.astype(F32)
            square = down * down
            lanes = square[:, 0:128]
            for q in range(1, 8):
                lanes = lanes + square[:, 128 * q : 128 * q + 128]
            squares[t, rows] = lanes
            return 0

        lax.fori_loop(0, BLOCK // SUB, body, 0, unroll=2)
        share(3, i, squares.at[t, rows_of(i)], squares.at[t, rows_of(i)])

    def final(i):
        arrived(3, i, squares.at[other, rows_of(i)])
        gain = gains[3:4, pl.ds(pl.multiple_of(t * HALF, HALF), HALF)]

        def body(k, _):
            rows = pl.ds(pl.multiple_of(i * BLOCK + k * SUB, SUB), SUB)
            inverse = mean_inverse(row_sum(squares[0, rows] + squares[1, rows]))
            add = (mixed[rows].astype(F32) * inverse * gain).astype(BF16).astype(F32)
            out[rows] = (x_buf[t, rows].astype(F32) + add).astype(BF16)
            return 0

        lax.fori_loop(0, BLOCK // SUB, body, 0, unroll=2)

    def round_(k):
        for b in range(NB):
            if 0 <= k - b <= 5:
                gather.tick(b, k - b)

    scales(0)
    fill()
    round_(1)
    scales(1)
    bands()
    scales(2)
    round_(2)
    for i in range(NR):
        first_norm(i)
    round_(3)
    scales(3)
    round_(4)
    scales(4)
    round_(5)
    scales(5)
    for c in range(4):
        mix(c)
    round_(6)
    for i in range(NR):
        pool(i)
        branch_share(i)
    for i in range(NR):
        middle(i)
    round_(7)
    for c in range(4):
        up(1, c)
    for c in range(4):
        up(2, c)
    round_(8)
    for i in range(2):
        down_first(i)
    round_(9)
    for i in range(NR):
        down_second(i, other, part_out)
        part_share(i)
    for i in range(NR):
        down_second(i, t, mixed)
    for i in range(NR):
        total(i)
    for i in range(NR):
        final(i)
    gather.finish()
    for copy in sent:
        copy.wait_send()


def on_device(
    tokens,
    norm_gains,
    mix_weight,
    mix_scale,
    group_weight,
    group_scale,
    up_weight,
    up_scale,
    down_weight,
    down_scale,
):
    place = lax.axis_index(FS)
    scales = jnp.concatenate([mix_scale, group_scale, up_scale, down_scale], axis=0)
    own = (jnp.arange(32, dtype=jnp.int32) == place)[None, None, :, None]
    tile = jnp.where(own, scales.reshape(40, 2, 1, 2), 0.0).reshape(40, 128)
    vmem = pl.BlockSpec(memory_space=pltpu.VMEM)
    dma = pltpu.SemaphoreType.DMA
    return pl.pallas_call(
        kernel,
        out_shape=jax.ShapeDtypeStruct((LENGTH, HALF), BF16),
        in_specs=[pl.BlockSpec(memory_space=pl.ANY)] + [vmem] * 6,
        out_specs=vmem,
        scratch_shapes=[pltpu.VMEM((2, 4, 4, r, 1024), BF16) for r in ROWS]
        + [
            pltpu.VMEM((2, LENGTH, HALF), BF16),
            pltpu.VMEM((LENGTH, 2 * HALF), BF16),
            pltpu.VMEM((LENGTH, HALF), BF16),
            pltpu.VMEM((2, LENGTH, HALF), BF16),
            pltpu.VMEM((LENGTH, 2048), BF16),
            pltpu.VMEM((2, LENGTH, HALF), F32),
            pltpu.VMEM((LENGTH, HALF), BF16),
            pltpu.VMEM((LENGTH, HALF), BF16),
            pltpu.VMEM((2, LENGTH, 128), F32),
            pltpu.VMEM((2, BLOCK, 2 * BLOCK), BF16),
            pltpu.VMEM((7, 40, 128), F32),
            pltpu.VMEM((2, 40, 128), F32),
            pltpu.VMEM((5, 1024), F32),
            dma((NB, 4, 10)),
            dma((NB, 4, 10)),
            dma((NR,)),
            dma((4, NR)),
            dma((4, NR)),
            dma((7,)),
            dma((7,)),
        ],
        compiler_params=pltpu.CompilerParams(
            collective_id=0, has_side_effects=True, vmem_limit_bytes=67_000_000
        ),
    )(tokens, norm_gains, mix_weight, group_weight, up_weight, down_weight, tile)


def solution(mesh):
    finer = Mesh(
        mesh.devices.reshape(mesh.shape["rep"], 2, 4, 4, mesh.shape["tp"]),
        ("rep", "fs_0", "fs_1", "fs_2", "tp"),
    )
    in_specs = (
        P(REP_FS, "tp"),
        P(),
        P(FS, "tp"),
        P("tp", FS),
        P("tp", FS, None),
        P("tp", FS),
        P(FS, "tp"),
        P("tp", FS),
        P("tp", FS),
        P("tp", FS),
    )
    out_specs = P(REP_FS, "tp")
    return jax.shard_map(
        on_device, mesh=finer, in_specs=in_specs, out_specs=out_specs, check_vma=False
    )
```

time: 561 us -> 135 us (0.24)
  waiting for transfers between devices: 295 us -> 0 us
  blocking collectives: 143 us -> 0 us
  Pallas kernels: 0 us -> 127 us
  matrix products: 37.3 us -> 0 us
  other arithmetic: 30.6 us -> 1.43 us
  local copies, waits for them, and re-layouts: 30.6 us -> 5.93 us
  between operations: 13.8 us -> 0.03 us
  starting transfers between devices: 9.67 us -> 0 us
    all_gather x6 -> x0, waiting for transfers between devices: 294 us -> none  [the longest x1 140 us: on_device(): lax.all_gather(down_weight.astype(jnp.bfloat16), FS, axis=1, tiled=True)]
    pallas_call x0 -> x1, Pallas kernels: none -> 127 us  [on_device(): pl.pallas_call(kernel, out_shape=jax.ShapeDtypeStruct((LENGTH, HALF), BF1...]
    all_gather x2 -> x0, blocking collectives: 87.4 us -> none  [the longest x1 68.3 us: rows_first(): out = lax.all_gather(both, axis, axis=0, tiled=True)]
    all_to_all x3 -> x0, blocking collectives: 55.6 us -> none  [the longest x2 27.9 us: sent_to_all(): return lax.all_to_all(copies, axis, split_axis=0, concat_axis=0, tiled=True)]
    dot_general x3 -> x0, matrix products: 37.3 us -> none  [the longest x1 25.6 us: on_device(): jnp.dot(hidden, down_whole, preferred_element_type=jnp.float32)]
    convert_element_type x11 -> x0, other arithmetic: 13.8 us -> none  [the longest x4 6.06 us: rounded(): values.astype(jnp.bfloat16)]
    reshape x3 -> x0, local copies, waits for them, and re-layouts: 11.4 us -> none  [the longest x1 5.56 us: on_device(): grouped.reshape(length, half_width) * group_cols.reshape(-1)]
    all_to_all x1 -> x0, starting transfers between devices: 9.21 us -> none  [sent_to_all(): return lax.all_to_all(copies, axis, split_axis=0, concat_axis=0, tiled=True)]
  transfers between devices with their start and end apart: 7 -> 0, of which waited for: 4 -> 0; matrix products, arithmetic and copies ran while one was open for 10% -> 0% of each run, Pallas kernels for 0% -> 0%
where the time goes in v1:
time: 135 us
  Pallas kernels  127 us (94%)
  local copies, waits for them, and re-layouts  5.93 us (4%)
  other arithmetic  1.43 us (1%)
    pallas_call x1, Pallas kernels, on_device(): pl.pallas_call(kernel, out_shape=jax.ShapeDtypeStruct((LENGTH, HALF), BF1...  127 us
    unnamed x2, local copies, waits for them, and re-layouts  5.43 us

profile of v1, /device:TPU:1, one launch (start us, length us, event | category | flops | bytes accessed | tf_op | source)
XLA Modules:
  0.0 134.7 jit_solution(18051247033477052910)
XLA Ops:
  0.0 0.8 pad_maximum_fusion
  0.8 0.1 broadcast_in_dim.29
  0.9 0.1 broadcast_in_dim.30
  1.0 0.1 broadcast_in_dim.32
  1.1 0.1 copy.13
  1.3 0.1 copy.14
  1.3 0.6 broadcast_select_fusion.tile
  2.0 2.4 %copy.15.down_w = f32[2048,64]{1,0:T(8,128)} copy(f32[2048,64]{0,1:T(8,128)} %param.18) | data formatting | bytes 1048576 | tf_op args[8]
  4.3 127.3 %shard_map.100 = bf16[1024,1024]{1,0:T(8,128)(2,1)} custom-call(bf16[1024,1024]{1,0:T(8,128)(2,1)} %tokens.1, f32[4,2048]{1,0:T(4,128)} %gains.1, f32[64,1024]{1,0:T(8,128)} %mix_w.1, f32[2,16,512]{2,1,0:T(8,128)} %group_w.1, f32[64,2048]{1,0:T(8,128)} %up_w.1, f32[2048,64]{1,0:T(8,128)} %copy.15.down_w, f32[40,128]{1,0:T(8,128)} %broadcast_select_fusion.tile), custom_call_target="tpu_custom_call" | custom-call | tf_op jit(solution)/shard_map/pallas_call | solution.py:487
  131.6 3.1 %copy.17 = bf16[1024,1024]{1,0:T(8,128)(2,1)} copy(bf16[1024,1024]{1,0:T(8,128)(2,1)} %shard_map.100) | data formatting | bytes 4194304
  (2 shorter events, 0.0 us)

commit v2 on v1

v2 whole, which is shorter than its diff:
```python
import functools

import jax
import jax.numpy as jnp
from jax import lax
from jax.experimental import pallas as pl
from jax.experimental.pallas import tpu as pltpu
from jax.sharding import Mesh
from jax.sharding import PartitionSpec as P

FS = ("fs_0", "fs_1", "fs_2")
REP_FS = ("rep", "fs_0", "fs_1", "fs_2")
MESH = pl.DeviceIdType.MESH
ALL = slice(None)
EPS = 1e-06

LENGTH = 1024
HALF = 1024
GW = 512
ROWS = (80, 64, 64, 64, 64)
BATCHES = ((0, 0, 256), (1, 0, 256), (2, 0, 256), (3, 0, 256), (4, 0, 128), (4, 512, 128))
NB = len(BATCHES)
POOL = 56
LAG = 20
MROWS = 512
BLOCK = 256
NR = LENGTH // BLOCK
F32, BF16 = jnp.float32, jnp.bfloat16


PLAN = (
    ("T", 1, 1, 0), ("T", 1, 0, 0), ("T", 1, 2, 0), ("T", 1, 3, 0), ("bands",), ("T", 3, 1, 0),
    ("T", 3, 0, 0), ("T", 3, 3, 0), ("T", 3, 2, 0), ("T", 4, 1, 0), ("T", 4, 0, 0), ("T", 5, 1, 0),
    ("T", 4, 2, 0), ("T", 4, 3, 0), ("T", 5, 0, 0), ("T", 5, 3, 0), ("T", 5, 2, 0), ("T", 2, 1, 0),
    ("T", 2, 0, 0), ("T", 0, 1, 1), ("T", 0, 0, 1), ("sc", 1), ("sc", 2), ("norm", 0), ("T", 0, 2, 1),
    ("T", 1, 1, 1), ("T", 0, 3, 1), ("T", 1, 0, 1), ("T", 2, 2, 0), ("T", 2, 3, 0), ("norm", 1),
    ("T", 1, 2, 1), ("T", 1, 3, 1), ("norm", 2), ("T", 3, 1, 1), ("T", 3, 0, 1), ("T", 3, 2, 1),
    ("T", 3, 3, 1), ("norm", 3), ("T", 4, 1, 1), ("T", 4, 0, 1), ("T", 4, 2, 1), ("T", 5, 1, 1),
    ("T", 4, 3, 1), ("T", 5, 0, 1), ("sc", 3), ("T", 5, 2, 1), ("T", 5, 3, 1), ("sc", 4), ("T", 2, 1, 1),
    ("T", 2, 0, 1), ("T", 0, 1, 2), ("T", 0, 0, 2), ("T", 1, 1, 2), ("T", 0, 2, 2), ("T", 0, 3, 2),
    ("T", 1, 0, 2), ("T", 1, 3, 2), ("T", 1, 2, 2), ("sc", 5), ("T", 3, 0, 2), ("T", 3, 1, 2),
    ("T", 3, 2, 2), ("T", 0, 2, 3), ("T", 3, 3, 2), ("T", 0, 0, 3), ("T", 0, 1, 3), ("T", 0, 3, 3),
    ("T", 4, 1, 2), ("T", 4, 0, 2), ("T", 4, 2, 2), ("T", 4, 3, 2), ("T", 5, 2, 2), ("T", 5, 3, 2),
    ("T", 1, 0, 3), ("T", 1, 1, 3), ("T", 1, 2, 3), ("T", 1, 3, 3), ("T", 0, 1, 4), ("T", 0, 2, 4),
    ("T", 0, 0, 4), ("T", 0, 3, 4), ("T", 2, 3, 1), ("T", 2, 2, 1), ("T", 1, 0, 4), ("T", 1, 1, 4),
    ("T", 2, 0, 2), ("T", 2, 1, 2), ("T", 0, 1, 5), ("mix", 1), ("T", 1, 2, 4), ("T", 1, 3, 4),
    ("T", 3, 0, 3), ("T", 3, 1, 3), ("T", 3, 2, 3), ("T", 3, 3, 3), ("T", 0, 0, 5), ("mix", 0),
    ("T", 2, 2, 2), ("T", 2, 3, 2), ("T", 0, 2, 5), ("mix", 2), ("T", 0, 3, 5), ("mix", 3), ("T", 2, 1, 3),
    ("T", 2, 0, 3), ("pool", 0), ("share", 0), ("pool", 1), ("share", 1), ("pool", 2), ("share", 2),
    ("pool", 3), ("T", 3, 1, 4), ("share", 3), ("mid", 0), ("T", 5, 1, 2), ("T", 5, 0, 2), ("T", 3, 0, 4),
    ("T", 5, 2, 3), ("T", 5, 3, 3), ("mid", 1), ("mid", 2), ("T", 2, 2, 3), ("T", 2, 3, 3), ("T", 2, 1, 4),
    ("mid", 3), ("T", 2, 0, 4), ("T", 3, 2, 4), ("T", 3, 3, 4), ("T", 1, 0, 5), ("up", 1, 0),
    ("T", 1, 1, 5), ("up", 1, 1), ("T", 1, 2, 5), ("up", 1, 2), ("T", 1, 3, 5), ("up", 1, 3),
    ("T", 4, 1, 3), ("T", 4, 0, 3), ("T", 2, 2, 4), ("T", 2, 3, 4), ("T", 4, 2, 3), ("T", 5, 1, 3),
    ("T", 4, 3, 3), ("T", 5, 0, 3), ("T", 5, 2, 4), ("T", 5, 3, 4), ("T", 3, 0, 5), ("T", 3, 1, 5),
    ("T", 3, 2, 5), ("T", 3, 3, 5), ("dn", 3, 0), ("dn", 3, 1), ("T", 4, 1, 4), ("T", 4, 0, 4),
    ("dn", 3, 2), ("T", 2, 1, 5), ("up", 2, 1), ("T", 2, 2, 5), ("up", 2, 2), ("T", 5, 1, 4),
    ("T", 2, 3, 5), ("up", 2, 3), ("T", 4, 2, 4), ("T", 4, 3, 4), ("T", 5, 0, 4), ("dn", 3, 3),
    ("T", 2, 0, 5), ("up", 2, 0), ("T", 4, 0, 5), ("T", 4, 1, 5), ("T", 4, 2, 5), ("T", 4, 3, 5),
    ("dn", 4, 0), ("dn", 4, 1), ("dn", 4, 2), ("dn", 4, 3), ("T", 5, 0, 5), ("T", 5, 1, 5), ("T", 5, 2, 5),
    ("T", 5, 3, 5), ("last", 0), ("last", 1), ("own", 0), ("total", 0), ("total", 1), ("own", 1),
    ("total", 2), ("total", 3), ("final", 0), ("final", 1), ("final", 2), ("final", 3),
)
ORDERS = (
    ("xyz", "yxz", "xzy", "yzx"),
    ("xyz", "yxz", "xzy", "yzx"),
    ("xyz", "yxz", "xzy", "yzx"),
    ("xyz", "yxz", "xzy", "yzx"),
    ("xzy", "yzx", "xzy", "yzx"),
    ("xyz", "yxz", "xzy", "yzx"),
)


def dot(a, b):
    return jnp.dot(a, b, preferred_element_type=F32)


def dot_t(a, b):
    return lax.dot_general(a, b, (((1,), (1,)), ((), ())), preferred_element_type=F32)


def spot():
    return dict(
        z=lax.axis_index("rep") * 2 + lax.axis_index("fs_0"),
        y=lax.axis_index("fs_1"),
        x=lax.axis_index("fs_2"),
        t=lax.axis_index("tp"),
    )


def to(axis, at):
    if axis == "x":
        return {"fs_2": at}
    if axis == "y":
        return {"fs_1": at}
    if axis == "z":
        return {"rep": at // 2, "fs_0": at % 2}
    return {"tp": at}


def send(src, dst, send_sem, recv_sem, axis, at):
    return pltpu.make_async_remote_copy(
        src_ref=src,
        dst_ref=dst,
        send_sem=send_sem,
        recv_sem=recv_sem,
        device_id=to(axis, at),
        device_id_type=MESH,
    )


class Gather:
    def __init__(self, bufs, send_sem, recv_sem, me):
        self.bufs, self.send_sem, self.recv_sem, self.me = bufs, send_sem, recv_sem, me
        self.sent, self.ticks, self.free = [], 0, list(range(POOL))
        self.steps = {
            (b, c): self.plan(b, c, order)
            for b in range(NB)
            for c, order in enumerate(ORDERS[b])
        }

    def region(self, b, c, at, half):
        buf, lane, width = BATCHES[b]
        lane, rows = lane + width * c, ALL
        if half is not None and width == 256:
            lane, width = lane + 128 * half, 128
        elif half is not None:
            rows = pl.ds(32 * half, 32)
        return self.bufs[buf].at[at["z"], at["y"], at["x"], rows, pl.ds(lane, width)]

    def copy(self, b, c, k, pool, src, dst, axis, at):
        recv_sem = self.recv_sem.at[b, c, k]
        return send(src, dst, self.send_sem.at[pool], recv_sem, axis, at)

    def plan(self, b, c, order):
        me = self.me
        own = dict(z=me["z"] % 2, y=me["y"], x=me["x"])
        steps = []
        for axis in order:
            up, down, far = (lax.rem(me[axis] + d, 4) for d in (1, 3, 2))

            def part(i, half=None, own=own, axis=axis):
                return self.region(b, c, {**own, axis: i}, half)

            if axis == "z":
                here, other = own["z"], 1 - own["z"]
                steps.append(([(part(here, 0), axis, up), (part(here, 1), axis, down)], part(other)))
            else:
                here = me[axis]
                two = self.region(b, c, {**own, axis: pl.ds(0, 2)}, None)
                steps.append(([(part(here), axis, up), (part(here), axis, down)], two))
                steps.append(([(part(down, 0), axis, up), (part(up, 1), axis, down)], part(far)))
            own = {**own, axis: ALL}
        return steps

    def tick(self, b, c, s):
        self.ticks += 1
        while self.sent and self.sent[0][0] < self.ticks - LAG:
            self.release()
        if s > 0:
            ref = self.steps[b, c][s - 1][1]
            self.copy(b, c, s - 1, 0, ref, ref, "x", self.me["x"]).wait_recv()
        if s < 5:
            for ref, axis, at in self.steps[b, c][s][0]:
                if not self.free:
                    self.release()
                pool = self.free.pop(0)
                copy = self.copy(b, c, s, pool, ref, ref, axis, at)
                copy.start()
                self.sent.append((self.ticks, pool, copy))

    def release(self):
        _, pool, copy = self.sent.pop(0)
        copy.wait_send()
        self.free.append(pool)

    def finish(self):
        while self.sent:
            self.release()


def greet(me, wait):
    barrier = pltpu.get_barrier_semaphore()
    peers = [("x", 1), ("x", 2), ("x", 3), ("y", 1), ("y", 2), ("y", 3), ("z", 1), ("z", 3)]
    if wait:
        pl.semaphore_wait(barrier, len(peers) + 1)
        return
    for axis, d in peers:
        pl.semaphore_signal(
            barrier, inc=1, device_id=to(axis, lax.rem(me[axis] + d, 4)), device_id_type=MESH
        )
    pl.semaphore_signal(barrier, inc=1, device_id=to("t", 1 - me["t"]), device_id_type=MESH)


def kernel(
    tokens,
    gains_in,
    mix_in,
    group_in,
    up_in,
    down_in,
    mix_s_in,
    group_s_in,
    up_s_in,
    down_s_in,
    out,
    gains,
    mix_w,
    group_w,
    up_w,
    down_w,
    mix_s,
    group_s,
    up_s,
    down_s,
    w0,
    w1,
    w2,
    w3,
    w4,
    x_buf,
    normed,
    mixed,
    branch,
    hidden,
    acc,
    part_out,
    part_in,
    squares,
    band,
    tile,
    sc_in,
    sc_sum,
    scale,
    inverses,
    g_send,
    g_recv,
    load_sem,
    p_send,
    p_recv,
    s_send,
    s_recv,
    out_sem,
):
    me = spot()
    greet(me, False)
    t, other = me["t"], 1 - me["t"]
    here = (me["z"] % 2, me["y"], me["x"])
    bufs = (w0, w1, w2, w3, w4)
    gather = Gather(bufs, g_send, g_recv, me)
    sent, outs = [], []

    def rows_of(i, size=BLOCK):
        return pl.ds(i * size, size)

    def scale_tile():
        place = me["z"] % 2 * 16 + me["y"] * 4 + me["x"]
        lane = lax.broadcasted_iota(jnp.int32, (1, 128), 1)
        base = 0
        for ref in (mix_s, group_s, up_s, down_s):
            n = ref.shape[1] // 2
            q = lax.broadcasted_iota(jnp.int32, (n, 2 * n), 0)
            r = lax.broadcasted_iota(jnp.int32, (n, 2 * n), 1)
            value = jnp.zeros((n, 128), F32)
            for j in range(2):
                for h in range(2):
                    own = jnp.where(r == 2 * q + h, ref[j : j + 1], 0.0)
                    column = jnp.sum(own, axis=1, keepdims=True)
                    value = value + jnp.where(lane == h * 64 + 2 * place + j, column, 0.0)
            tile[base : base + n] = value
            base += n

    def load(k, src, dst):
        copy = pltpu.make_async_copy(src, dst, load_sem.at[k])
        copy.start()
        return copy

    pairs = (
        (mix_in, mix_w),
        (group_in, group_w),
        (mix_s_in, mix_s),
        (group_s_in, group_s),
        (up_s_in, up_s),
        (down_s_in, down_s),
        (up_in, up_w),
        (down_in, down_w),
        (gains_in, gains),
    )
    early = [load(k, src, dst) for k, (src, dst) in enumerate(pairs)]
    loads = [
        load(len(pairs) + i, tokens.at[rows_of(i)], x_buf.at[t, rows_of(i)]) for i in range(NR)
    ]
    for copy in early[:6]:
        copy.wait()
    w0[here[0], here[1], here[2], 0:64] = mix_w[...].astype(BF16)
    w0[here[0], here[1], here[2], 64:80, 0:GW] = group_w[0].astype(BF16)
    w0[here[0], here[1], here[2], 64:80, GW:] = group_w[1].astype(BF16)
    scale_tile()
    for copy in early[6:]:
        copy.wait()
    up_all, down_all = up_w[...].astype(BF16), down_w[...].astype(BF16)
    for ref, lane in ((w1, 0), (w2, 1024)):
        ref[here[0], here[1], here[2]] = up_all[:, lane : lane + 1024]
    for ref, lane in ((w3, 0), (w4, 1024)):
        ref[here[0], here[1], here[2]] = down_all[:, lane : lane + 1024]
    with jax.named_scope("greet"):
        greet(me, True)

    def share(kind, i, src, dst):
        copy = send(src, dst, p_send.at[kind, i], p_recv.at[kind, i], "t", other)
        copy.start()
        sent.append(copy)

    def arrived(kind, i, ref):
        send(ref, ref, p_send.at[kind, i], p_recv.at[kind, i], "t", other).wait_recv()

    for c in range(4):
        gather.tick(0, c, 0)
    for i in range(NR):
        share(0, i, tokens.at[rows_of(i)], x_buf.at[t, rows_of(i)])

    def scale_send(slot, src, axis, at):
        copy = send(src, sc_in.at[slot], s_send.at[slot], s_recv.at[slot], axis, at)
        copy.start()
        sent.append(copy)

    def scale_wait(slot):
        send(sc_in.at[slot], sc_in.at[slot], s_send.at[slot], s_recv.at[slot], "t", other).wait_recv()

    def scales(step):
        if step == 0:
            for d in (1, 2, 3):
                scale_send(d - 1, tile, "x", lax.rem(me["x"] + d, 4))
        if step == 1:
            for d in (1, 2, 3):
                scale_wait(d - 1)
            sc_sum[0] = tile[...] + sc_in[0] + sc_in[1] + sc_in[2]
        if step == 2:
            for d in (1, 2, 3):
                scale_send(d + 2, sc_sum.at[0], "y", lax.rem(me["y"] + d, 4))
        if step == 3:
            for d in (1, 2, 3):
                scale_wait(d + 2)
            sc_sum[1] = sc_sum[0] + sc_in[3] + sc_in[4] + sc_in[5]
        if step == 4:
            scale_send(6, sc_sum.at[1], "z", me["z"] + 1 - 2 * (me["z"] % 2))
        if step == 5:
            scale_wait(6)
            whole = sc_sum[1] + sc_in[6]
            for q in range(40):
                scale[q // 8 : q // 8 + 1, 128 * (q % 8) : 128 * (q % 8) + 128] = whole[q : q + 1]

    def bands():
        i = lax.broadcasted_iota(jnp.int32, (BLOCK, 2 * BLOCK), 0)
        j = lax.broadcasted_iota(jnp.int32, (BLOCK, 2 * BLOCK), 1) - BLOCK
        for g, window in enumerate((2 + 6 * t, 4 + 12 * t)):
            band[g] = jnp.where((j <= i) & (j > i - window), 1.0, 0.0).astype(BF16)

    def mean_inverse(total):
        return lax.rsqrt(total * (1.0 / (2 * HALF)) + EPS)

    def row_sum(v):
        return jnp.sum(v, axis=1, keepdims=True)

    SUB = 16

    def first_norm(i):
        loads[i].wait()
        arrived(0, i, x_buf.at[other, rows_of(i)])
        g0, g1 = gains[0:1, 0:HALF], gains[0:1, HALF:]

        def body(k, _):
            rows = pl.ds(pl.multiple_of(i * BLOCK + k * SUB, SUB), SUB)
            a, b = x_buf[0, rows].astype(F32), x_buf[1, rows].astype(F32)
            inverse = mean_inverse(row_sum(a * a + b * b))
            normed[rows, 0:HALF] = (a * inverse * g0).astype(BF16)
            normed[rows, HALF:] = (b * inverse * g1).astype(BF16)
            return 0

        lax.fori_loop(0, BLOCK // SUB, body, 0, unroll=2)

    def mix(c):
        cols = slice(256 * c, 256 * c + 256)
        weight = w0[:, :, :, 0:64, cols].reshape(2 * HALF, 256)

        def body(i, _):
            rows = pl.ds(pl.multiple_of(i * MROWS, MROWS), MROWS)
            mixed[rows, cols] = (dot(normed[rows], weight) * scale[0:1, cols]).astype(BF16)
            return 0

        lax.fori_loop(0, LENGTH // MROWS, body, 0)

    def pool(i):
        rows = slice(i * BLOCK, i * BLOCK + BLOCK)
        for g in range(2):
            cols = slice(GW * g, GW * g + GW)
            window = (2 + 6 * t, 4 + 12 * t)[g]
            own = mixed[rows, cols]
            if i == 0:
                sums = dot(band[g, :, BLOCK:], own)
                position = lax.broadcasted_iota(jnp.int32, (BLOCK, 1), 0)
                sums = sums / jnp.minimum(position + 1, window).astype(F32)
            else:
                sums = dot(band[g], mixed[rows.start - BLOCK : rows.stop, cols])
                sums = sums * (1.0 / jnp.full((BLOCK, 1), window, jnp.int32).astype(F32))
            pooled = (sums - own.astype(F32)).astype(BF16)
            weight = w0[:, :, :, 64:80, cols].reshape(GW, GW)
            branch[t, rows, cols] = (dot(pooled, weight) * scale[1:2, cols]).astype(BF16)

    def branch_share(i):
        share(1, i, branch.at[t, rows_of(i)], branch.at[t, rows_of(i)])

    def middle(i):
        arrived(1, i, branch.at[other, rows_of(i)])
        post = [gains[1:2, 0:HALF], gains[1:2, HALF:]]
        pre = [gains[2:3, 0:HALF], gains[2:3, HALF:]]

        def body(k, _):
            rows = pl.ds(pl.multiple_of(i * BLOCK + k * SUB, SUB), SUB)
            parts = [branch[h, rows].astype(F32) for h in range(2)]
            inverse = mean_inverse(row_sum(parts[0] * parts[0] + parts[1] * parts[1]))
            mids = []
            for h in range(2):
                add = (parts[h] * inverse * post[h]).astype(BF16).astype(F32)
                mid = (x_buf[h, rows].astype(F32) + add).astype(BF16)
                x_buf[h, rows] = mid
                mids.append(mid.astype(F32))
            inverse = mean_inverse(row_sum(mids[0] * mids[0] + mids[1] * mids[1]))
            for h in range(2):
                normed[rows, h * HALF : h * HALF + HALF] = (mids[h] * inverse * pre[h]).astype(BF16)
            return 0

        lax.fori_loop(0, BLOCK // SUB, body, 0, unroll=2)

    def up(b, c):
        cols = slice(256 * c, 256 * c + 256)
        place = slice((b - 1) * 1024 + 256 * c, (b - 1) * 1024 + 256 * c + 256)
        weight = bufs[b][:, :, :, :, cols].reshape(2 * HALF, 256)

        def body(i, _):
            rows = pl.ds(pl.multiple_of(i * MROWS, MROWS), MROWS)
            act = jnp.maximum(dot(normed[rows], weight) * scale[b + 1 : b + 2, cols], 0.0)
            hidden[rows, place] = (act * act).astype(BF16)
            return 0

        lax.fori_loop(0, LENGTH // MROWS, body, 0)

    def down(b, n, part=None):
        buf, lane, width = BATCHES[b]
        half, k = (other, n) if n < 2 else (t, n - 2)
        first = (buf - 3) * 1024 + lane
        weight = bufs[buf][half, 2 * k : 2 * k + 2, :, :, lane : lane + 4 * width]
        weight = weight.reshape(512, 4 * width)
        cols = slice(512 * k, 512 * k + 512)

        def body(i, _):
            rows = pl.ds(pl.multiple_of(i * MROWS, MROWS), MROWS)
            value = dot_t(hidden[rows, first : first + 4 * width], weight)
            if b > 3:
                value = value + acc[half, rows, cols]
            if b < NB - 1:
                acc[half, rows, cols] = value
            elif n < 2:
                part_out[rows, cols] = value.astype(BF16)
            else:
                mixed[rows, cols] = value.astype(BF16)
            return 0

        if part is not None:
            body(part, 0)
        else:
            lax.fori_loop(0, LENGTH // MROWS, body, 0)

    def last(part):
        for n in range(2):
            down(NB - 1, n, part)
        share(2, part, part_out.at[rows_of(part, 512)], part_in.at[rows_of(part, 512)])

    def last_own(part):
        for n in range(2, 4):
            down(NB - 1, n, part)

    def total(i):
        if i % 2 == 0:
            arrived(2, i // 2, part_in.at[rows_of(i // 2, 512)])

        def body(k, _):
            rows = pl.ds(pl.multiple_of(i * BLOCK + k * SUB, SUB), SUB)
            both = mixed[rows].astype(F32) + part_in[rows].astype(F32)
            value = (both * scale[4:5]).astype(BF16)
            mixed[rows] = value
            value = value.astype(F32)
            square = value * value
            lanes = square[:, 0:128]
            for q in range(1, 8):
                lanes = lanes + square[:, 128 * q : 128 * q + 128]
            squares[t, rows] = lanes
            return 0

        lax.fori_loop(0, BLOCK // SUB, body, 0, unroll=2)
        share(3, i, squares.at[t, rows_of(i)], squares.at[t, rows_of(i)])

    def final(i):
        arrived(3, i, squares.at[other, rows_of(i)])
        gain = gains[3:4, pl.ds(pl.multiple_of(t * HALF, HALF), HALF)]
        squared = squares[0, rows_of(i)] + squares[1, rows_of(i)]
        inverses[...] = jnp.broadcast_to(mean_inverse(row_sum(squared)), (BLOCK, 128))

        def body(k, _):
            at = pl.ds(pl.multiple_of(k * SUB, SUB), SUB)
            rows = pl.ds(pl.multiple_of(i * BLOCK + k * SUB, SUB), SUB)
            inverse = jnp.concatenate([inverses[at]] * (HALF // 128), axis=1)
            add = (mixed[rows].astype(F32) * inverse * gain).astype(BF16).astype(F32)
            mixed[rows] = (x_buf[t, rows].astype(F32) + add).astype(BF16)
            return 0

        lax.fori_loop(0, BLOCK // SUB, body, 0, unroll=2)
        copy = pltpu.make_async_copy(mixed.at[rows_of(i)], out.at[rows_of(i)], out_sem.at[i])
        copy.start()
        outs.append(copy)

    def run(name, step, *args):
        with jax.named_scope(name):
            step(*args)

    steps = dict(
        sc=scales, bands=bands, norm=first_norm, mix=mix, pool=pool, mid=middle, up=up, dn=down
    )
    steps.update(T=gather.tick, share=branch_share, total=total, final=final)
    steps.update(last=last, own=last_own)
    run("sc", scales, 0)
    for name, *args in PLAN:
        run("#".join(map(str, (name, *args))), steps[name], *args)
    with jax.named_scope("finish"):
        gather.finish()
        for copy in sent:
            copy.wait_send()
    with jax.named_scope("outs"):
        for copy in outs:
            copy.wait()


def on_device(
    tokens,
    norm_gains,
    mix_weight,
    mix_scale,
    group_weight,
    group_scale,
    up_weight,
    up_scale,
    down_weight,
    down_scale,
):
    arrays = (tokens, norm_gains, mix_weight, group_weight, up_weight, down_weight.T)
    arrays += (mix_scale.T, group_scale.T, up_scale.T, down_scale.T)
    dma = pltpu.SemaphoreType.DMA
    return pl.pallas_call(
        kernel,
        out_shape=jax.ShapeDtypeStruct((LENGTH, HALF), BF16),
        in_specs=[pl.BlockSpec(memory_space=pl.ANY)] + [pl.BlockSpec(memory_space=pl.ANY)] * 9,
        out_specs=pl.BlockSpec(memory_space=pl.ANY),
        scratch_shapes=[pltpu.VMEM(a.shape, F32) for a in arrays[1:]]
        + [pltpu.VMEM((2, 4, 4, r, 1024), BF16) for r in ROWS]
        + [
            pltpu.VMEM((2, LENGTH, HALF), BF16),
            pltpu.VMEM((LENGTH, 2 * HALF), BF16),
            pltpu.VMEM((LENGTH, HALF), BF16),
            pltpu.VMEM((2, LENGTH, HALF), BF16),
            pltpu.VMEM((LENGTH, 2048), BF16),
            pltpu.VMEM((2, LENGTH, HALF), F32),
            pltpu.VMEM((LENGTH, HALF), BF16),
            pltpu.VMEM((LENGTH, HALF), BF16),
            pltpu.VMEM((2, LENGTH, 128), F32),
            pltpu.VMEM((2, BLOCK, 2 * BLOCK), BF16),
            pltpu.VMEM((40, 128), F32),
            pltpu.VMEM((7, 40, 128), F32),
            pltpu.VMEM((2, 40, 128), F32),
            pltpu.VMEM((5, 1024), F32),
            pltpu.VMEM((BLOCK, 128), F32),
            dma((POOL,)),
            dma((NB, 4, 5)),
            dma((9 + NR,)),
            dma((4, NR)),
            dma((4, NR)),
            dma((7,)),
            dma((7,)),
            dma((NR,)),
        ],
        compiler_params=pltpu.CompilerParams(
            collective_id=0, has_side_effects=True, vmem_limit_bytes=67_000_000
        ),
    )(*arrays)


def solution(mesh):
    finer = Mesh(
        mesh.devices.reshape(mesh.shape["rep"], 2, 4, 4, mesh.shape["tp"]),
        ("rep", "fs_0", "fs_1", "fs_2", "tp"),
    )
    in_specs = (
        P(REP_FS, "tp"),
        P(),
        P(FS, "tp"),
        P("tp", FS),
        P("tp", FS, None),
        P("tp", FS),
        P(FS, "tp"),
        P("tp", FS),
        P("tp", FS),
        P("tp", FS),
    )
    out_specs = P(REP_FS, "tp")
    return jax.shard_map(
        on_device, mesh=finer, in_specs=in_specs, out_specs=out_specs, check_vma=False
    )
```

time: 135 us -> 110 us (0.81)
  Pallas kernels: 127 us -> 107 us
  local copies, waits for them, and re-layouts: 5.93 us -> 3.08 us
  other arithmetic: 1.43 us -> 0 us
    pallas_call x1, Pallas kernels: 127 us -> 107 us  [on_device(): pl.pallas_call(kernel, out_shape=jax.ShapeDtypeStruct((LENGTH, HALF), BF1...]
    unnamed x2 -> x1, local copies, waits for them, and re-layouts: 5.43 us -> 3.08 us
where the time goes in v2:
time: 110 us
  Pallas kernels  107 us (97%)
  local copies, waits for them, and re-layouts  3.08 us (3%)
    pallas_call x1, Pallas kernels, on_device(): pl.pallas_call(kernel, out_shape=jax.ShapeDtypeStruct((LENGTH, HALF), BF1...  107 us
    unnamed x1, local copies, waits for them, and re-layouts  3.08 us

profile of v2, /device:TPU:1, one launch (start us, length us, event | category | flops | bytes accessed | tf_op | source)
XLA Modules:
  0.0 109.6 jit_solution(17943542832786617877)
XLA Ops:
  0.0 106.5 %shard_map.100 = bf16[1024,1024]{1,0:T(8,128)(2,1)} custom-call(bf16[1024,1024]{1,0:T(8,128)(2,1)} %tokens.1, f32[4,2048]{1,0:T(4,128)} %gains_in.1, f32[64,1024]{1,0:T(8,128)} %mix_in.1, f32[2,16,512]{2,1,0:T(8,128)} %group_in.1, f32[64,2048]{1,0:T(8,128)} %up_in.1, f32[64,2048]{1,0:T(8,128)} %bitcast.5, f32[2,16]{1,0:T(2,128)} %bitcast.6, ...), custom_call_target="tpu_custom_call" | custom-call | tf_op jit(solution)/shard_map/pallas_call | solution.py:558
  106.5 3.1 %copy.12 = bf16[1024,1024]{1,0:T(8,128)(2,1)} copy(bf16[1024,1024]{1,0:T(8,128)(2,1)} %shard_map.100) | data formatting | bytes 4194304

commit v3 on v2

--- a/solution.py
+++ b/solution.py
@@ -18,10 +18,18 @@
 HALF = 1024
 GW = 512
 ROWS = (80, 64, 64, 64, 64)
-BATCHES = ((0, 0, 256), (1, 0, 256), (2, 0, 256), (3, 0, 256), (4, 0, 128), (4, 512, 128))
+BATCHES = (
+    (0, 0, 64, 0, 256),
+    (0, 64, 16, 0, 256),
+    (1, 0, 64, 0, 256),
+    (2, 0, 64, 0, 256),
+    (3, 0, 64, 0, 256),
+    (4, 0, 64, 0, 128),
+    (4, 0, 64, 512, 128),
+)
 NB = len(BATCHES)
-POOL = 56
-LAG = 20
+POOL = 44
+LAG = 10
 MROWS = 512
 BLOCK = 256
 NR = LENGTH // BLOCK
@@ -29,45 +37,35 @@
 
 
 PLAN = (
-    ("T", 1, 1, 0), ("T", 1, 0, 0), ("T", 1, 2, 0), ("T", 1, 3, 0), ("bands",), ("T", 3, 1, 0),
-    ("T", 3, 0, 0), ("T", 3, 3, 0), ("T", 3, 2, 0), ("T", 4, 1, 0), ("T", 4, 0, 0), ("T", 5, 1, 0),
-    ("T", 4, 2, 0), ("T", 4, 3, 0), ("T", 5, 0, 0), ("T", 5, 3, 0), ("T", 5, 2, 0), ("T", 2, 1, 0),
-    ("T", 2, 0, 0), ("T", 0, 1, 1), ("T", 0, 0, 1), ("sc", 1), ("sc", 2), ("norm", 0), ("T", 0, 2, 1),
-    ("T", 1, 1, 1), ("T", 0, 3, 1), ("T", 1, 0, 1), ("T", 2, 2, 0), ("T", 2, 3, 0), ("norm", 1),
-    ("T", 1, 2, 1), ("T", 1, 3, 1), ("norm", 2), ("T", 3, 1, 1), ("T", 3, 0, 1), ("T", 3, 2, 1),
-    ("T", 3, 3, 1), ("norm", 3), ("T", 4, 1, 1), ("T", 4, 0, 1), ("T", 4, 2, 1), ("T", 5, 1, 1),
-    ("T", 4, 3, 1), ("T", 5, 0, 1), ("sc", 3), ("T", 5, 2, 1), ("T", 5, 3, 1), ("sc", 4), ("T", 2, 1, 1),
-    ("T", 2, 0, 1), ("T", 0, 1, 2), ("T", 0, 0, 2), ("T", 1, 1, 2), ("T", 0, 2, 2), ("T", 0, 3, 2),
-    ("T", 1, 0, 2), ("T", 1, 3, 2), ("T", 1, 2, 2), ("sc", 5), ("T", 3, 0, 2), ("T", 3, 1, 2),
-    ("T", 3, 2, 2), ("T", 0, 2, 3), ("T", 3, 3, 2), ("T", 0, 0, 3), ("T", 0, 1, 3), ("T", 0, 3, 3),
-    ("T", 4, 1, 2), ("T", 4, 0, 2), ("T", 4, 2, 2), ("T", 4, 3, 2), ("T", 5, 2, 2), ("T", 5, 3, 2),
-    ("T", 1, 0, 3), ("T", 1, 1, 3), ("T", 1, 2, 3), ("T", 1, 3, 3), ("T", 0, 1, 4), ("T", 0, 2, 4),
-    ("T", 0, 0, 4), ("T", 0, 3, 4), ("T", 2, 3, 1), ("T", 2, 2, 1), ("T", 1, 0, 4), ("T", 1, 1, 4),
-    ("T", 2, 0, 2), ("T", 2, 1, 2), ("T", 0, 1, 5), ("mix", 1), ("T", 1, 2, 4), ("T", 1, 3, 4),
-    ("T", 3, 0, 3), ("T", 3, 1, 3), ("T", 3, 2, 3), ("T", 3, 3, 3), ("T", 0, 0, 5), ("mix", 0),
-    ("T", 2, 2, 2), ("T", 2, 3, 2), ("T", 0, 2, 5), ("mix", 2), ("T", 0, 3, 5), ("mix", 3), ("T", 2, 1, 3),
-    ("T", 2, 0, 3), ("pool", 0), ("share", 0), ("pool", 1), ("share", 1), ("pool", 2), ("share", 2),
-    ("pool", 3), ("T", 3, 1, 4), ("share", 3), ("mid", 0), ("T", 5, 1, 2), ("T", 5, 0, 2), ("T", 3, 0, 4),
-    ("T", 5, 2, 3), ("T", 5, 3, 3), ("mid", 1), ("mid", 2), ("T", 2, 2, 3), ("T", 2, 3, 3), ("T", 2, 1, 4),
-    ("mid", 3), ("T", 2, 0, 4), ("T", 3, 2, 4), ("T", 3, 3, 4), ("T", 1, 0, 5), ("up", 1, 0),
-    ("T", 1, 1, 5), ("up", 1, 1), ("T", 1, 2, 5), ("up", 1, 2), ("T", 1, 3, 5), ("up", 1, 3),
-    ("T", 4, 1, 3), ("T", 4, 0, 3), ("T", 2, 2, 4), ("T", 2, 3, 4), ("T", 4, 2, 3), ("T", 5, 1, 3),
-    ("T", 4, 3, 3), ("T", 5, 0, 3), ("T", 5, 2, 4), ("T", 5, 3, 4), ("T", 3, 0, 5), ("T", 3, 1, 5),
-    ("T", 3, 2, 5), ("T", 3, 3, 5), ("dn", 3, 0), ("dn", 3, 1), ("T", 4, 1, 4), ("T", 4, 0, 4),
-    ("dn", 3, 2), ("T", 2, 1, 5), ("up", 2, 1), ("T", 2, 2, 5), ("up", 2, 2), ("T", 5, 1, 4),
-    ("T", 2, 3, 5), ("up", 2, 3), ("T", 4, 2, 4), ("T", 4, 3, 4), ("T", 5, 0, 4), ("dn", 3, 3),
-    ("T", 2, 0, 5), ("up", 2, 0), ("T", 4, 0, 5), ("T", 4, 1, 5), ("T", 4, 2, 5), ("T", 4, 3, 5),
-    ("dn", 4, 0), ("dn", 4, 1), ("dn", 4, 2), ("dn", 4, 3), ("T", 5, 0, 5), ("T", 5, 1, 5), ("T", 5, 2, 5),
-    ("T", 5, 3, 5), ("last", 0), ("last", 1), ("own", 0), ("total", 0), ("total", 1), ("own", 1),
-    ("total", 2), ("total", 3), ("final", 0), ("final", 1), ("final", 2), ("final", 3),
+    ("T", 1, 0, 0), ("T", 1, 1, 0), ("T", 3, 0, 0), ("T", 2, 0, 0), ("T", 3, 1, 0), ("T", 2, 1, 0),
+    ("T", 4, 0, 0), ("bands",), ("T", 4, 1, 0), ("T", 5, 0, 0), ("T", 5, 1, 0), ("T", 6, 0, 0),
+    ("T", 6, 1, 0), ("T", 0, 0, 1), ("sc", 1), ("sc", 2), ("T", 0, 1, 1), ("norm", 0), ("T", 1, 0, 1),
+    ("T", 1, 1, 1), ("norm", 1), ("T", 3, 0, 1), ("T", 2, 0, 1), ("norm", 2), ("T", 3, 1, 1), ("norm", 3),
+    ("T", 2, 1, 1), ("T", 4, 0, 1), ("sc", 3), ("T", 4, 1, 1), ("sc", 4), ("T", 5, 0, 1), ("T", 5, 1, 1),
+    ("T", 6, 0, 1), ("T", 6, 1, 1), ("T", 0, 0, 2), ("T", 0, 1, 2), ("T", 1, 0, 2), ("T", 1, 1, 2),
+    ("T", 3, 0, 2), ("T", 3, 1, 2), ("T", 2, 0, 2), ("sc", 5), ("T", 4, 1, 2), ("T", 4, 0, 2),
+    ("T", 5, 1, 2), ("T", 0, 0, 3), ("T", 0, 1, 3), ("T", 6, 0, 2), ("T", 1, 0, 3), ("T", 1, 1, 3),
+    ("T", 6, 1, 2), ("T", 2, 1, 2), ("T", 0, 0, 4), ("T", 5, 0, 2), ("T", 4, 0, 3), ("T", 4, 1, 3),
+    ("T", 0, 1, 4), ("T", 2, 0, 3), ("T", 2, 1, 3), ("T", 1, 0, 4), ("T", 1, 1, 4), ("T", 3, 0, 3),
+    ("T", 3, 1, 3), ("T", 4, 0, 4), ("T", 0, 0, 5), ("mix", 0), ("T", 0, 1, 5), ("mix", 1), ("T", 2, 0, 4),
+    ("T", 2, 1, 4), ("T", 4, 1, 4), ("T", 1, 0, 5), ("T", 1, 1, 5), ("pool", 0), ("share", 0), ("pool", 1),
+    ("T", 3, 0, 4), ("share", 1), ("pool", 2), ("share", 2), ("pool", 3), ("share", 3), ("mid", 0),
+    ("T", 6, 0, 3), ("mid", 1), ("mid", 2), ("T", 5, 0, 3), ("T", 3, 1, 4), ("T", 5, 1, 3), ("T", 6, 1, 3),
+    ("mid", 3), ("T", 2, 0, 5), ("up", 1, 0), ("T", 2, 1, 5), ("up", 1, 1), ("T", 6, 0, 4), ("T", 4, 0, 5),
+    ("T", 4, 1, 5), ("dn", 4, 0), ("T", 5, 0, 4), ("dn", 4, 1), ("dn", 4, 2), ("T", 3, 1, 5), ("up", 2, 1),
+    ("T", 5, 1, 4), ("T", 3, 0, 5), ("up", 2, 0), ("T", 6, 1, 4), ("dn", 4, 3), ("T", 5, 0, 5),
+    ("T", 5, 1, 5), ("dn", 5, 0), ("dn", 5, 1), ("dn", 5, 2), ("dn", 5, 3), ("T", 6, 0, 5), ("T", 6, 1, 5),
+    ("last", 0), ("last", 1), ("own", 0), ("total", 0), ("total", 1), ("own", 1), ("total", 2),
+    ("total", 3), ("final", 0), ("final", 1), ("final", 2), ("final", 3),
 )
 ORDERS = (
-    ("xyz", "yxz", "xzy", "yzx"),
-    ("xyz", "yxz", "xzy", "yzx"),
-    ("xyz", "yxz", "xzy", "yzx"),
-    ("xyz", "yxz", "xzy", "yzx"),
-    ("xzy", "yzx", "xzy", "yzx"),
-    ("xyz", "yxz", "xzy", "yzx"),
+    ("xyz", "xzy"),
+    ("xzy", "xzy"),
+    ("xyz", "xzy"),
+    ("xyz", "xzy"),
+    ("xyz", "xzy"),
+    ("xyz", "xzy"),
+    ("xzy", "xzy"),
 )
 
 
@@ -114,58 +112,62 @@
         self.bufs, self.send_sem, self.recv_sem, self.me = bufs, send_sem, recv_sem, me
         self.sent, self.ticks, self.free = [], 0, list(range(POOL))
         self.steps = {
-            (b, c): self.plan(b, c, order)
-            for b in range(NB)
-            for c, order in enumerate(ORDERS[b])
+            (b, p): self.plan(b, p, order) for b in range(NB) for p, order in enumerate(ORDERS[b])
         }
 
-    def region(self, b, c, at, half):
-        buf, lane, width = BATCHES[b]
-        lane, rows = lane + width * c, ALL
+    def region(self, b, c, at, half=None, colours=1):
+        buf, row, rows, lane, width = BATCHES[b]
+        lane, width = lane + width * c, width * colours
         if half is not None and width == 256:
             lane, width = lane + 128 * half, 128
         elif half is not None:
-            rows = pl.ds(32 * half, 32)
-        return self.bufs[buf].at[at["z"], at["y"], at["x"], rows, pl.ds(lane, width)]
-
-    def copy(self, b, c, k, pool, src, dst, axis, at):
-        recv_sem = self.recv_sem.at[b, c, k]
-        return send(src, dst, self.send_sem.at[pool], recv_sem, axis, at)
-
-    def plan(self, b, c, order):
+            row, rows = row + rows // 2 * half, rows // 2
+        return self.bufs[buf].at[at["z"], at["y"], at["x"], pl.ds(row, rows), pl.ds(lane, width)]
+
+    def plan(self, b, p, order):
         me = self.me
-        own = dict(z=me["z"] % 2, y=me["y"], x=me["x"])
+        owns = [dict(z=me["z"] % 2, y=me["y"], x=me["x"])] * 2
         steps = []
         for axis in order:
-            up, down, far = (lax.rem(me[axis] + d, 4) for d in (1, 3, 2))
-
-            def part(i, half=None, own=own, axis=axis):
-                return self.region(b, c, {**own, axis: i}, half)
-
             if axis == "z":
-                here, other = own["z"], 1 - own["z"]
-                steps.append(([(part(here, 0), axis, up), (part(here, 1), axis, down)], part(other)))
+                copies = []
+                for k, d in enumerate((1, 3)):
+                    ref = self.region(b, 2 * p + k, owns[k])
+                    copies.append((ref, "z", lax.rem(me["z"] + d, 4)))
+                steps.append((copies, self.region(b, 2 * p, owns[0], colours=2)))
             else:
-                here = me[axis]
-                two = self.region(b, c, {**own, axis: pl.ds(0, 2)}, None)
-                steps.append(([(part(here), axis, up), (part(here), axis, down)], two))
-                steps.append(([(part(down, 0), axis, up), (part(up, 1), axis, down)], part(far)))
-            own = {**own, axis: ALL}
+                first, second = [], []
+                for k in range(2):
+                    along = axis if k == 0 else {"x": "y", "y": "x"}[axis]
+                    up, down = lax.rem(me[along] + 1, 4), lax.rem(me[along] + 3, 4)
+
+                    def part(i, half=None):
+                        return self.region(b, 2 * p + k, {**owns[k], along: i}, half)
+
+                    first += [(part(me[along]), along, up), (part(me[along]), along, down)]
+                    second += [(part(down, 0), along, up), (part(up, 1), along, down)]
+                two = self.region(b, 2 * p, {**owns[0], axis: pl.ds(0, 2)}, colours=2)
+                steps.append((first, two))
+                steps.append((second, self.region(b, 2 * p, owns[0], colours=2)))
+            owns = [{**own, axis if k == 0 else {"x": "y", "y": "x", "z": "z"}[axis]: ALL} for k, own in enumerate(owns)]
         return steps
 
-    def tick(self, b, c, s):
+    def copy(self, b, p, k, pool, ref, axis, at):
+        return send(ref, ref, self.send_sem.at[pool], self.recv_sem.at[b, p, k], axis, at)
+
+    def tick(self, b, p, s):
         self.ticks += 1
         while self.sent and self.sent[0][0] < self.ticks - LAG:
             self.release()
         if s > 0:
-            ref = self.steps[b, c][s - 1][1]
-            self.copy(b, c, s - 1, 0, ref, ref, "x", self.me["x"]).wait_recv()
+            ref = self.steps[b, p][s - 1][1]
+            self.copy(b, p, s - 1, 0, ref, "x", self.me["x"]).wait_recv()
         if s < 5:
-            for ref, axis, at in self.steps[b, c][s][0]:
+            for ref, axis, at in self.steps[b, p][s][0]:
                 if not self.free:
                     self.release()
                 pool = self.free.pop(0)
-                copy = self.copy(b, c, s, pool, ref, ref, axis, at)
+                copy = self.copy(b, p, s, pool, ref, axis, at)
                 copy.start()
                 self.sent.append((self.ticks, pool, copy))
 
@@ -240,7 +242,6 @@
     p_recv,
     s_send,
     s_recv,
-    out_sem,
 ):
     me = spot()
     greet(me, False)
@@ -248,7 +249,7 @@
     here = (me["z"] % 2, me["y"], me["x"])
     bufs = (w0, w1, w2, w3, w4)
     gather = Gather(bufs, g_send, g_recv, me)
-    sent, outs = [], []
+    sent = []
 
     def rows_of(i, size=BLOCK):
         return pl.ds(i * size, size)
@@ -314,8 +315,8 @@
     def arrived(kind, i, ref):
         send(ref, ref, p_send.at[kind, i], p_recv.at[kind, i], "t", other).wait_recv()
 
-    for c in range(4):
-        gather.tick(0, c, 0)
+    for p in range(2):
+        gather.tick(0, p, 0)
     for i in range(NR):
         share(0, i, tokens.at[rows_of(i)], x_buf.at[t, rows_of(i)])
 
@@ -362,7 +363,7 @@
     def row_sum(v):
         return jnp.sum(v, axis=1, keepdims=True)
 
-    SUB = 16
+    SUB, UNROLL = 16, 4
 
     def first_norm(i):
         loads[i].wait()
@@ -377,18 +378,12 @@
             normed[rows, HALF:] = (b * inverse * g1).astype(BF16)
             return 0
 
-        lax.fori_loop(0, BLOCK // SUB, body, 0, unroll=2)
-
-    def mix(c):
-        cols = slice(256 * c, 256 * c + 256)
-        weight = w0[:, :, :, 0:64, cols].reshape(2 * HALF, 256)
-
-        def body(i, _):
-            rows = pl.ds(pl.multiple_of(i * MROWS, MROWS), MROWS)
-            mixed[rows, cols] = (dot(normed[rows], weight) * scale[0:1, cols]).astype(BF16)
-            return 0
-
-        lax.fori_loop(0, LENGTH // MROWS, body, 0)
+        lax.fori_loop(0, BLOCK // SUB, body, 0, unroll=UNROLL)
+
+    def mix(p):
+        cols = slice(GW * p, GW * p + GW)
+        weight = w0[:, :, :, 0:64, cols].reshape(2 * HALF, GW)
+        mixed[:, cols] = (dot(normed[...], weight) * scale[0:1, cols]).astype(BF16)
 
     def pool(i):
         rows = slice(i * BLOCK, i * BLOCK + BLOCK)
@@ -430,23 +425,17 @@
                 normed[rows, h * HALF : h * HALF + HALF] = (mids[h] * inverse * pre[h]).astype(BF16)
             return 0
 
-        lax.fori_loop(0, BLOCK // SUB, body, 0, unroll=2)
-
-    def up(b, c):
-        cols = slice(256 * c, 256 * c + 256)
-        place = slice((b - 1) * 1024 + 256 * c, (b - 1) * 1024 + 256 * c + 256)
-        weight = bufs[b][:, :, :, :, cols].reshape(2 * HALF, 256)
-
-        def body(i, _):
-            rows = pl.ds(pl.multiple_of(i * MROWS, MROWS), MROWS)
-            act = jnp.maximum(dot(normed[rows], weight) * scale[b + 1 : b + 2, cols], 0.0)
-            hidden[rows, place] = (act * act).astype(BF16)
-            return 0
-
-        lax.fori_loop(0, LENGTH // MROWS, body, 0)
+        lax.fori_loop(0, BLOCK // SUB, body, 0, unroll=UNROLL)
+
+    def up(buf, p):
+        cols = slice(512 * p, 512 * p + 512)
+        place = slice((buf - 1) * 1024 + 512 * p, (buf - 1) * 1024 + 512 * p + 512)
+        weight = bufs[buf][:, :, :, :, cols].reshape(2 * HALF, 512)
+        act = jnp.maximum(dot(normed[...], weight) * scale[buf + 1 : buf + 2, cols], 0.0)
+        hidden[:, place] = (act * act).astype(BF16)
 
     def down(b, n, part=None):
-        buf, lane, width = BATCHES[b]
+        buf, _, _, lane, width = BATCHES[b]
         half, k = (other, n) if n < 2 else (t, n - 2)
         first = (buf - 3) * 1024 + lane
         weight = bufs[buf][half, 2 * k : 2 * k + 2, :, :, lane : lane + 4 * width]
@@ -456,7 +445,7 @@
         def body(i, _):
             rows = pl.ds(pl.multiple_of(i * MROWS, MROWS), MROWS)
             value = dot_t(hidden[rows, first : first + 4 * width], weight)
-            if b > 3:
+            if buf > 3:
                 value = value + acc[half, rows, cols]
             if b < NB - 1:
                 acc[half, rows, cols] = value
@@ -497,7 +486,7 @@
             squares[t, rows] = lanes
             return 0
 
-        lax.fori_loop(0, BLOCK // SUB, body, 0, unroll=2)
+        lax.fori_loop(0, BLOCK // SUB, body, 0, unroll=UNROLL)
         share(3, i, squares.at[t, rows_of(i)], squares.at[t, rows_of(i)])
 
     def final(i):
@@ -511,13 +500,10 @@
             rows = pl.ds(pl.multiple_of(i * BLOCK + k * SUB, SUB), SUB)
             inverse = jnp.concatenate([inverses[at]] * (HALF // 128), axis=1)
             add = (mixed[rows].astype(F32) * inverse * gain).astype(BF16).astype(F32)
-            mixed[rows] = (x_buf[t, rows].astype(F32) + add).astype(BF16)
+            out[rows] = (x_buf[t, rows].astype(F32) + add).astype(BF16)
             return 0
 
-        lax.fori_loop(0, BLOCK // SUB, body, 0, unroll=2)
-        copy = pltpu.make_async_copy(mixed.at[rows_of(i)], out.at[rows_of(i)], out_sem.at[i])
-        copy.start()
-        outs.append(copy)
+        lax.fori_loop(0, BLOCK // SUB, body, 0, unroll=UNROLL)
 
     def run(name, step, *args):
         with jax.named_scope(name):
@@ -535,9 +521,6 @@
         gather.finish()
         for copy in sent:
             copy.wait_send()
-    with jax.named_scope("outs"):
-        for copy in outs:
-            copy.wait()
 
 
 def on_device(
@@ -557,9 +540,9 @@
     dma = pltpu.SemaphoreType.DMA
     return pl.pallas_call(
         kernel,
-        out_shape=jax.ShapeDtypeStruct((LENGTH, HALF), BF16),
+        out_shape=pltpu.VMEM((LENGTH, HALF), BF16),
         in_specs=[pl.BlockSpec(memory_space=pl.ANY)] + [pl.BlockSpec(memory_space=pl.ANY)] * 9,
-        out_specs=pl.BlockSpec(memory_space=pl.ANY),
+        out_specs=pl.BlockSpec(memory_space=pltpu.VMEM),
         scratch_shapes=[pltpu.VMEM(a.shape, F32) for a in arrays[1:]]
         + [pltpu.VMEM((2, 4, 4, r, 1024), BF16) for r in ROWS]
         + [
@@ -579,16 +562,15 @@
             pltpu.VMEM((5, 1024), F32),
             pltpu.VMEM((BLOCK, 128), F32),
             dma((POOL,)),
-            dma((NB, 4, 5)),
+            dma((NB, 2, 5)),
             dma((9 + NR,)),
             dma((4, NR)),
             dma((4, NR)),
             dma((7,)),
             dma((7,)),
-            dma((NR,)),
         ],
         compiler_params=pltpu.CompilerParams(
-            collective_id=0, has_side_effects=True, vmem_limit_bytes=67_000_000
+            collective_id=0, has_side_effects=True, vmem_limit_bytes=60_000_000
         ),
     )(*arrays)
 

time: 110 us -> 105 us (0.955)
  Pallas kernels: 107 us -> 103 us
  local copies, waits for them, and re-layouts: 3.08 us -> 1.32 us
    pallas_call x1, Pallas kernels: 107 us -> 103 us  [on_device(): pl.pallas_call(kernel, out_shape=pltpu.VMEM((LENGTH, HALF), BF16), in_spe...]
    unnamed x1, local copies, waits for them, and re-layouts: 3.08 us -> 1.32 us
where the time goes in v3:
time: 105 us
  Pallas kernels  103 us (98%)
  local copies, waits for them, and re-layouts  1.32 us (1%)
    pallas_call x1, Pallas kernels, on_device(): pl.pallas_call(kernel, out_shape=pltpu.VMEM((LENGTH, HALF), BF16), in_spe...  103 us

profile of v3, /device:TPU:1, one launch (start us, length us, event | category | flops | bytes accessed | tf_op | source)
XLA Modules:
  0.0 104.7 jit_solution(16927967833694107769)
XLA Ops:
  0.0 103.3 %shard_map.100 = bf16[1024,1024]{1,0:T(8,128)(2,1)S(1)} custom-call(bf16[1024,1024]{1,0:T(8,128)(2,1)} %tokens.1, f32[4,2048]{1,0:T(4,128)} %gains_in.1, f32[64,1024]{1,0:T(8,128)} %mix_in.1, f32[2,16,512]{2,1,0:T(8,128)} %group_in.1, f32[64,2048]{1,0:T(8,128)} %up_in.1, f32[64,2048]{1,0:T(8,128)} %bitcast.5, f32[2,16]{1,0:T(2,128)} %bitcast.6, ...), custom_call_target="tpu_custom_call" | custom-call | tf_op jit(solution)/shard_map/pallas_call | solution.py:541
  103.3 1.3 %copy.12 = bf16[1024,1024]{1,0:T(8,128)(2,1)} copy(bf16[1024,1024]{1,0:T(8,128)(2,1)S(1)} %shard_map.100) | data formatting | bytes 4194304

commit v4 on v3

--- a/solution.py
+++ b/solution.py
@@ -18,18 +18,18 @@
 HALF = 1024
 GW = 512
 ROWS = (80, 64, 64, 64, 64)
+KCUT = 512
 BATCHES = (
-    (0, 0, 64, 0, 256),
-    (0, 64, 16, 0, 256),
-    (1, 0, 64, 0, 256),
-    (2, 0, 64, 0, 256),
-    (3, 0, 64, 0, 256),
-    (4, 0, 64, 0, 128),
-    (4, 0, 64, 512, 128),
+    (0, 0, 64, 0, 256, 0, 256),
+    (0, 64, 16, 0, 256, 0, 256),
+    (1, 0, 64, 0, 256, 0, 256),
+    (2, 0, 64, 0, 256, 0, 256),
+    (3, 0, 64, 0, 256, 0, 256),
+    (4, 0, 16, 0, KCUT, 16, 0),
+    (4, 0, 16, KCUT, 1024 - KCUT, 16, 0),
 )
 NB = len(BATCHES)
-POOL = 44
-LAG = 10
+POOL = 54
 MROWS = 512
 BLOCK = 256
 NR = LENGTH // BLOCK
@@ -37,35 +37,35 @@
 
 
 PLAN = (
-    ("T", 1, 0, 0), ("T", 1, 1, 0), ("T", 3, 0, 0), ("T", 2, 0, 0), ("T", 3, 1, 0), ("T", 2, 1, 0),
-    ("T", 4, 0, 0), ("bands",), ("T", 4, 1, 0), ("T", 5, 0, 0), ("T", 5, 1, 0), ("T", 6, 0, 0),
-    ("T", 6, 1, 0), ("T", 0, 0, 1), ("sc", 1), ("sc", 2), ("T", 0, 1, 1), ("norm", 0), ("T", 1, 0, 1),
-    ("T", 1, 1, 1), ("norm", 1), ("T", 3, 0, 1), ("T", 2, 0, 1), ("norm", 2), ("T", 3, 1, 1), ("norm", 3),
-    ("T", 2, 1, 1), ("T", 4, 0, 1), ("sc", 3), ("T", 4, 1, 1), ("sc", 4), ("T", 5, 0, 1), ("T", 5, 1, 1),
-    ("T", 6, 0, 1), ("T", 6, 1, 1), ("T", 0, 0, 2), ("T", 0, 1, 2), ("T", 1, 0, 2), ("T", 1, 1, 2),
-    ("T", 3, 0, 2), ("T", 3, 1, 2), ("T", 2, 0, 2), ("sc", 5), ("T", 4, 1, 2), ("T", 4, 0, 2),
-    ("T", 5, 1, 2), ("T", 0, 0, 3), ("T", 0, 1, 3), ("T", 6, 0, 2), ("T", 1, 0, 3), ("T", 1, 1, 3),
-    ("T", 6, 1, 2), ("T", 2, 1, 2), ("T", 0, 0, 4), ("T", 5, 0, 2), ("T", 4, 0, 3), ("T", 4, 1, 3),
-    ("T", 0, 1, 4), ("T", 2, 0, 3), ("T", 2, 1, 3), ("T", 1, 0, 4), ("T", 1, 1, 4), ("T", 3, 0, 3),
-    ("T", 3, 1, 3), ("T", 4, 0, 4), ("T", 0, 0, 5), ("mix", 0), ("T", 0, 1, 5), ("mix", 1), ("T", 2, 0, 4),
-    ("T", 2, 1, 4), ("T", 4, 1, 4), ("T", 1, 0, 5), ("T", 1, 1, 5), ("pool", 0), ("share", 0), ("pool", 1),
-    ("T", 3, 0, 4), ("share", 1), ("pool", 2), ("share", 2), ("pool", 3), ("share", 3), ("mid", 0),
-    ("T", 6, 0, 3), ("mid", 1), ("mid", 2), ("T", 5, 0, 3), ("T", 3, 1, 4), ("T", 5, 1, 3), ("T", 6, 1, 3),
-    ("mid", 3), ("T", 2, 0, 5), ("up", 1, 0), ("T", 2, 1, 5), ("up", 1, 1), ("T", 6, 0, 4), ("T", 4, 0, 5),
-    ("T", 4, 1, 5), ("dn", 4, 0), ("T", 5, 0, 4), ("dn", 4, 1), ("dn", 4, 2), ("T", 3, 1, 5), ("up", 2, 1),
-    ("T", 5, 1, 4), ("T", 3, 0, 5), ("up", 2, 0), ("T", 6, 1, 4), ("dn", 4, 3), ("T", 5, 0, 5),
-    ("T", 5, 1, 5), ("dn", 5, 0), ("dn", 5, 1), ("dn", 5, 2), ("dn", 5, 3), ("T", 6, 0, 5), ("T", 6, 1, 5),
-    ("last", 0), ("last", 1), ("own", 0), ("total", 0), ("total", 1), ("own", 1), ("total", 2),
-    ("total", 3), ("final", 0), ("final", 1), ("final", 2), ("final", 3),
+    ("T", 1, 1, 0), ("T", 1, 0, 0), ("T", 3, 0, 0), ("T", 2, 1, 0), ("T", 5, 0, 0), ("T", 6, 0, 0),
+    ("T", 4, 1, 0), ("T", 2, 0, 0), ("T", 0, 1, 1), ("T", 0, 0, 1), ("sc", 1), ("T", 3, 1, 0),
+    ("T", 4, 0, 0), ("T", 1, 0, 1), ("T", 5, 0, 1), ("T", 3, 0, 1), ("T", 2, 1, 1), ("T", 6, 1, 0),
+    ("sc", 2), ("T", 2, 0, 1), ("T", 0, 1, 2), ("T", 1, 1, 1), ("T", 4, 1, 1), ("bands",), ("T", 0, 0, 2),
+    ("T", 1, 0, 2), ("norm", 0), ("T", 5, 0, 2), ("norm", 1), ("T", 2, 1, 2), ("norm", 3), ("T", 3, 1, 1),
+    ("T", 1, 1, 2), ("T", 6, 0, 1), ("T", 2, 0, 2), ("T", 0, 0, 3), ("T", 4, 1, 2), ("T", 3, 1, 2),
+    ("T", 5, 1, 0), ("T", 1, 0, 3), ("T", 4, 0, 1), ("T", 3, 0, 2), ("T", 1, 1, 3), ("norm", 2),
+    ("T", 0, 0, 4), ("T", 6, 1, 1), ("T", 0, 1, 3), ("T", 5, 0, 3), ("T", 1, 0, 4), ("T", 3, 0, 3),
+    ("sc", 3), ("T", 4, 0, 2), ("T", 5, 1, 1), ("sc", 4), ("T", 2, 0, 3), ("T", 1, 1, 4), ("T", 0, 1, 4),
+    ("T", 5, 1, 2), ("T", 4, 0, 3), ("T", 4, 1, 3), ("T", 0, 0, 5), ("T", 2, 1, 3), ("T", 1, 0, 5),
+    ("sc", 5), ("T", 6, 0, 2), ("T", 3, 1, 3), ("T", 2, 0, 4), ("T", 0, 1, 5), ("mix", 0), ("T", 1, 1, 5),
+    ("T", 4, 0, 4), ("mix", 1), ("pool", 0), ("pool", 1), ("share", 1), ("T", 3, 0, 4), ("pool", 2),
+    ("share", 0), ("mid", 0), ("T", 2, 0, 5), ("pool", 3), ("share", 3), ("T", 2, 1, 4), ("share", 2),
+    ("T", 6, 0, 3), ("mid", 2), ("T", 4, 1, 4), ("T", 6, 1, 2), ("mid", 1), ("T", 5, 1, 3), ("mid", 3),
+    ("up", 1, 0), ("T", 4, 0, 5), ("T", 3, 1, 4), ("T", 2, 1, 5), ("up", 1, 1), ("T", 4, 1, 5),
+    ("dn", 4, 3), ("T", 6, 0, 4), ("T", 6, 1, 3), ("dn", 4, 2), ("T", 5, 1, 4), ("dn", 4, 1), ("dn", 4, 0),
+    ("T", 5, 0, 4), ("T", 3, 1, 5), ("up", 2, 1), ("T", 3, 0, 5), ("T", 6, 1, 4), ("up", 2, 0),
+    ("T", 5, 1, 5), ("T", 5, 0, 5), ("dn", 5, 2), ("dn", 5, 0), ("dn", 5, 1), ("dn", 5, 3), ("T", 6, 0, 5),
+    ("T", 6, 1, 5), ("last", 0), ("last", 1), ("own", 0), ("total", 0), ("total", 1), ("own", 1),
+    ("total", 2), ("total", 3), ("final", 0), ("final", 1), ("final", 2), ("final", 3),
 )
 ORDERS = (
     ("xyz", "xzy"),
-    ("xzy", "xzy"),
-    ("xyz", "xzy"),
+    ("xyz", "xyz"),
     ("xyz", "xzy"),
     ("xyz", "xzy"),
     ("xyz", "xzy"),
     ("xzy", "xzy"),
+    ("xyz", "zxy"),
 )
 
 
@@ -110,18 +110,17 @@
 class Gather:
     def __init__(self, bufs, send_sem, recv_sem, me):
         self.bufs, self.send_sem, self.recv_sem, self.me = bufs, send_sem, recv_sem, me
-        self.sent, self.ticks, self.free = [], 0, list(range(POOL))
+        self.on_way, self.unused = {}, list(range(POOL))
         self.steps = {
             (b, p): self.plan(b, p, order) for b in range(NB) for p, order in enumerate(ORDERS[b])
         }
 
     def region(self, b, c, at, half=None, colours=1):
-        buf, row, rows, lane, width = BATCHES[b]
-        lane, width = lane + width * c, width * colours
-        if half is not None and width == 256:
-            lane, width = lane + 128 * half, 128
-        elif half is not None:
-            row, rows = row + rows // 2 * half, rows // 2
+        buf, row, rows, lane, width, row_step, step = BATCHES[b]
+        row, lane = row + row_step * c, lane + step * c
+        rows, width = rows + row_step * (colours - 1), width + step * (colours - 1)
+        if half is not None:
+            lane, width = lane + width // 2 * half, width // 2
         return self.bufs[buf].at[at["z"], at["y"], at["x"], pl.ds(row, rows), pl.ds(lane, width)]
 
     def plan(self, b, p, order):
@@ -152,33 +151,25 @@
             owns = [{**own, axis if k == 0 else {"x": "y", "y": "x", "z": "z"}[axis]: ALL} for k, own in enumerate(owns)]
         return steps
 
-    def copy(self, b, p, k, pool, ref, axis, at):
-        return send(ref, ref, self.send_sem.at[pool], self.recv_sem.at[b, p, k], axis, at)
+    def start(self, key, src, dst, recv_sem, axis, at):
+        pool = self.unused.pop(0)
+        copy = send(src, dst, self.send_sem.at[pool], recv_sem, axis, at)
+        copy.start()
+        self.on_way.setdefault(key, []).append((pool, copy))
+
+    def arrived(self, key, ref, recv_sem):
+        send(ref, ref, self.send_sem.at[0], recv_sem, "t", 1 - self.me["t"]).wait_recv()
+        for pool, copy in self.on_way.pop(key):
+            copy.wait_send()
+            self.unused.append(pool)
 
     def tick(self, b, p, s):
-        self.ticks += 1
-        while self.sent and self.sent[0][0] < self.ticks - LAG:
-            self.release()
         if s > 0:
             ref = self.steps[b, p][s - 1][1]
-            self.copy(b, p, s - 1, 0, ref, "x", self.me["x"]).wait_recv()
+            self.arrived((b, p, s - 1), ref, self.recv_sem.at[b, p, s - 1])
         if s < 5:
             for ref, axis, at in self.steps[b, p][s][0]:
-                if not self.free:
-                    self.release()
-                pool = self.free.pop(0)
-                copy = self.copy(b, p, s, pool, ref, axis, at)
-                copy.start()
-                self.sent.append((self.ticks, pool, copy))
-
-    def release(self):
-        _, pool, copy = self.sent.pop(0)
-        copy.wait_send()
-        self.free.append(pool)
-
-    def finish(self):
-        while self.sent:
-            self.release()
+                self.start((b, p, s), ref, ref, self.recv_sem.at[b, p, s], axis, at)
 
 
 def greet(me, wait):
@@ -238,9 +229,7 @@
     g_send,
     g_recv,
     load_sem,
-    p_send,
     p_recv,
-    s_send,
     s_recv,
 ):
     me = spot()
@@ -249,7 +238,6 @@
     here = (me["z"] % 2, me["y"], me["x"])
     bufs = (w0, w1, w2, w3, w4)
     gather = Gather(bufs, g_send, g_recv, me)
-    sent = []
 
     def rows_of(i, size=BLOCK):
         return pl.ds(i * size, size)
@@ -288,9 +276,7 @@
         (gains_in, gains),
     )
     early = [load(k, src, dst) for k, (src, dst) in enumerate(pairs)]
-    loads = [
-        load(len(pairs) + i, tokens.at[rows_of(i)], x_buf.at[t, rows_of(i)]) for i in range(NR)
-    ]
+    own_tokens = load(len(pairs), tokens, x_buf.at[t])
     for copy in early[:6]:
         copy.wait()
     w0[here[0], here[1], here[2], 0:64] = mix_w[...].astype(BF16)
@@ -308,45 +294,35 @@
         greet(me, True)
 
     def share(kind, i, src, dst):
-        copy = send(src, dst, p_send.at[kind, i], p_recv.at[kind, i], "t", other)
-        copy.start()
-        sent.append(copy)
+        gather.start((kind, i), src, dst, p_recv.at[kind, i], "t", other)
 
     def arrived(kind, i, ref):
-        send(ref, ref, p_send.at[kind, i], p_recv.at[kind, i], "t", other).wait_recv()
+        gather.arrived((kind, i), ref, p_recv.at[kind, i])
 
     for p in range(2):
         gather.tick(0, p, 0)
-    for i in range(NR):
-        share(0, i, tokens.at[rows_of(i)], x_buf.at[t, rows_of(i)])
-
-    def scale_send(slot, src, axis, at):
-        copy = send(src, sc_in.at[slot], s_send.at[slot], s_recv.at[slot], axis, at)
-        copy.start()
-        sent.append(copy)
-
-    def scale_wait(slot):
-        send(sc_in.at[slot], sc_in.at[slot], s_send.at[slot], s_recv.at[slot], "t", other).wait_recv()
+    share(0, 0, tokens, x_buf.at[t])
 
     def scales(step):
         if step == 0:
             for d in (1, 2, 3):
-                scale_send(d - 1, tile, "x", lax.rem(me["x"] + d, 4))
+                at = lax.rem(me["x"] + d, 4)
+                gather.start("sx", tile, sc_in.at[d - 1], s_recv.at[0], "x", at)
         if step == 1:
-            for d in (1, 2, 3):
-                scale_wait(d - 1)
+            gather.arrived("sx", sc_in.at[0:3], s_recv.at[0])
             sc_sum[0] = tile[...] + sc_in[0] + sc_in[1] + sc_in[2]
         if step == 2:
             for d in (1, 2, 3):
-                scale_send(d + 2, sc_sum.at[0], "y", lax.rem(me["y"] + d, 4))
+                at = lax.rem(me["y"] + d, 4)
+                gather.start("sy", sc_sum.at[0], sc_in.at[d + 2], s_recv.at[1], "y", at)
         if step == 3:
-            for d in (1, 2, 3):
-                scale_wait(d + 2)
+            gather.arrived("sy", sc_in.at[3:6], s_recv.at[1])
             sc_sum[1] = sc_sum[0] + sc_in[3] + sc_in[4] + sc_in[5]
         if step == 4:
-            scale_send(6, sc_sum.at[1], "z", me["z"] + 1 - 2 * (me["z"] % 2))
+            at = me["z"] + 1 - 2 * (me["z"] % 2)
+            gather.start("sz", sc_sum.at[1], sc_in.at[6], s_recv.at[2], "z", at)
         if step == 5:
-            scale_wait(6)
+            gather.arrived("sz", sc_in.at[6], s_recv.at[2])
             whole = sc_sum[1] + sc_in[6]
             for q in range(40):
                 scale[q // 8 : q // 8 + 1, 128 * (q % 8) : 128 * (q % 8) + 128] = whole[q : q + 1]
@@ -366,8 +342,9 @@
     SUB, UNROLL = 16, 4
 
     def first_norm(i):
-        loads[i].wait()
-        arrived(0, i, x_buf.at[other, rows_of(i)])
+        if i == 0:
+            own_tokens.wait()
+            arrived(0, 0, x_buf.at[other])
         g0, g1 = gains[0:1, 0:HALF], gains[0:1, HALF:]
 
         def body(k, _):
@@ -435,16 +412,16 @@
         hidden[:, place] = (act * act).astype(BF16)
 
     def down(b, n, part=None):
-        buf, _, _, lane, width = BATCHES[b]
+        buf, lane, width = ((3, 0, 1024), (4, 0, KCUT), (4, KCUT, 1024 - KCUT))[b - 4]
         half, k = (other, n) if n < 2 else (t, n - 2)
         first = (buf - 3) * 1024 + lane
-        weight = bufs[buf][half, 2 * k : 2 * k + 2, :, :, lane : lane + 4 * width]
-        weight = weight.reshape(512, 4 * width)
+        weight = bufs[buf][half, 2 * k : 2 * k + 2, :, :, lane : lane + width]
+        weight = weight.reshape(512, width)
         cols = slice(512 * k, 512 * k + 512)
 
         def body(i, _):
             rows = pl.ds(pl.multiple_of(i * MROWS, MROWS), MROWS)
-            value = dot_t(hidden[rows, first : first + 4 * width], weight)
+            value = dot_t(hidden[rows, first : first + width], weight)
             if buf > 3:
                 value = value + acc[half, rows, cols]
             if b < NB - 1:
@@ -517,10 +494,6 @@
     run("sc", scales, 0)
     for name, *args in PLAN:
         run("#".join(map(str, (name, *args))), steps[name], *args)
-    with jax.named_scope("finish"):
-        gather.finish()
-        for copy in sent:
-            copy.wait_send()
 
 
 def on_device(
@@ -563,11 +536,9 @@
             pltpu.VMEM((BLOCK, 128), F32),
             dma((POOL,)),
             dma((NB, 2, 5)),
-            dma((9 + NR,)),
+            dma((10,)),
             dma((4, NR)),
-            dma((4, NR)),
-            dma((7,)),
-            dma((7,)),
+            dma((3,)),
         ],
         compiler_params=pltpu.CompilerParams(
             collective_id=0, has_side_effects=True, vmem_limit_bytes=60_000_000

time: 105 us -> 102 us (0.971)
  Pallas kernels: 103 us -> 101 us
    pallas_call x1, Pallas kernels: 103 us -> 101 us  [on_device(): pl.pallas_call(kernel, out_shape=pltpu.VMEM((LENGTH, HALF), BF16), in_spe...]
where the time goes in v4:
time: 102 us
  Pallas kernels  101 us (99%)
  local copies, waits for them, and re-layouts  1.32 us (1%)
    pallas_call x1, Pallas kernels, on_device(): pl.pallas_call(kernel, out_shape=pltpu.VMEM((LENGTH, HALF), BF16), in_spe...  101 us

profile of v4, /device:TPU:1, one launch (start us, length us, event | category | flops | bytes accessed | tf_op | source)
XLA Modules:
  0.0 102.1 jit_solution(8572523659452819321)
XLA Ops:
  0.0 100.8 %shard_map.100 = bf16[1024,1024]{1,0:T(8,128)(2,1)S(1)} custom-call(bf16[1024,1024]{1,0:T(8,128)(2,1)} %tokens.1, f32[4,2048]{1,0:T(4,128)} %gains_in.1, f32[64,1024]{1,0:T(8,128)} %mix_in.1, f32[2,16,512]{2,1,0:T(8,128)} %group_in.1, f32[64,2048]{1,0:T(8,128)} %up_in.1, f32[64,2048]{1,0:T(8,128)} %bitcast.5, f32[2,16]{1,0:T(2,128)} %bitcast.6, ...), custom_call_target="tpu_custom_call" | custom-call | tf_op jit(solution)/shard_map/pallas_call | solution.py:514
  100.8 1.3 %copy.12 = bf16[1024,1024]{1,0:T(8,128)(2,1)} copy(bf16[1024,1024]{1,0:T(8,128)(2,1)S(1)} %shard_map.100) | data formatting | bytes 4194304

commit v5 on v4

--- a/solution.py
+++ b/solution.py
@@ -29,7 +29,7 @@
     (4, 0, 16, KCUT, 1024 - KCUT, 16, 0),
 )
 NB = len(BATCHES)
-POOL = 54
+POOL = 16
 MROWS = 512
 BLOCK = 256
 NR = LENGTH // BLOCK
@@ -37,35 +37,35 @@
 
 
 PLAN = (
-    ("T", 1, 1, 0), ("T", 1, 0, 0), ("T", 3, 0, 0), ("T", 2, 1, 0), ("T", 5, 0, 0), ("T", 6, 0, 0),
-    ("T", 4, 1, 0), ("T", 2, 0, 0), ("T", 0, 1, 1), ("T", 0, 0, 1), ("sc", 1), ("T", 3, 1, 0),
-    ("T", 4, 0, 0), ("T", 1, 0, 1), ("T", 5, 0, 1), ("T", 3, 0, 1), ("T", 2, 1, 1), ("T", 6, 1, 0),
-    ("sc", 2), ("T", 2, 0, 1), ("T", 0, 1, 2), ("T", 1, 1, 1), ("T", 4, 1, 1), ("bands",), ("T", 0, 0, 2),
-    ("T", 1, 0, 2), ("norm", 0), ("T", 5, 0, 2), ("norm", 1), ("T", 2, 1, 2), ("norm", 3), ("T", 3, 1, 1),
-    ("T", 1, 1, 2), ("T", 6, 0, 1), ("T", 2, 0, 2), ("T", 0, 0, 3), ("T", 4, 1, 2), ("T", 3, 1, 2),
-    ("T", 5, 1, 0), ("T", 1, 0, 3), ("T", 4, 0, 1), ("T", 3, 0, 2), ("T", 1, 1, 3), ("norm", 2),
-    ("T", 0, 0, 4), ("T", 6, 1, 1), ("T", 0, 1, 3), ("T", 5, 0, 3), ("T", 1, 0, 4), ("T", 3, 0, 3),
-    ("sc", 3), ("T", 4, 0, 2), ("T", 5, 1, 1), ("sc", 4), ("T", 2, 0, 3), ("T", 1, 1, 4), ("T", 0, 1, 4),
-    ("T", 5, 1, 2), ("T", 4, 0, 3), ("T", 4, 1, 3), ("T", 0, 0, 5), ("T", 2, 1, 3), ("T", 1, 0, 5),
-    ("sc", 5), ("T", 6, 0, 2), ("T", 3, 1, 3), ("T", 2, 0, 4), ("T", 0, 1, 5), ("mix", 0), ("T", 1, 1, 5),
-    ("T", 4, 0, 4), ("mix", 1), ("pool", 0), ("pool", 1), ("share", 1), ("T", 3, 0, 4), ("pool", 2),
-    ("share", 0), ("mid", 0), ("T", 2, 0, 5), ("pool", 3), ("share", 3), ("T", 2, 1, 4), ("share", 2),
-    ("T", 6, 0, 3), ("mid", 2), ("T", 4, 1, 4), ("T", 6, 1, 2), ("mid", 1), ("T", 5, 1, 3), ("mid", 3),
-    ("up", 1, 0), ("T", 4, 0, 5), ("T", 3, 1, 4), ("T", 2, 1, 5), ("up", 1, 1), ("T", 4, 1, 5),
-    ("dn", 4, 3), ("T", 6, 0, 4), ("T", 6, 1, 3), ("dn", 4, 2), ("T", 5, 1, 4), ("dn", 4, 1), ("dn", 4, 0),
-    ("T", 5, 0, 4), ("T", 3, 1, 5), ("up", 2, 1), ("T", 3, 0, 5), ("T", 6, 1, 4), ("up", 2, 0),
-    ("T", 5, 1, 5), ("T", 5, 0, 5), ("dn", 5, 2), ("dn", 5, 0), ("dn", 5, 1), ("dn", 5, 3), ("T", 6, 0, 5),
-    ("T", 6, 1, 5), ("last", 0), ("last", 1), ("own", 0), ("total", 0), ("total", 1), ("own", 1),
-    ("total", 2), ("total", 3), ("final", 0), ("final", 1), ("final", 2), ("final", 3),
+    ("bands",), ("T", 2, 0, 0), ("T", 1, 0, 0), ("T", 1, 1, 0), ("T", 6, 0, 0), ("T", 5, 0, 0),
+    ("T", 4, 0, 0), ("T", 5, 1, 0), ("T", 4, 1, 0), ("T", 3, 1, 0), ("T", 0, 0, 1), ("sc", 1), ("sc", 2),
+    ("T", 0, 1, 1), ("T", 2, 1, 0), ("T", 6, 1, 0), ("T", 3, 0, 0), ("T", 5, 0, 1), ("T", 1, 1, 1),
+    ("T", 4, 0, 1), ("T", 6, 0, 1), ("T", 2, 0, 1), ("T", 1, 0, 1), ("T", 4, 1, 1), ("norm", 0),
+    ("T", 3, 1, 1), ("T", 0, 0, 2), ("T", 5, 1, 1), ("T", 0, 1, 2), ("T", 3, 0, 1), ("norm", 1),
+    ("T", 5, 0, 2), ("T", 6, 1, 1), ("norm", 3), ("T", 1, 1, 2), ("T", 1, 0, 2), ("T", 4, 1, 2), ("sc", 3),
+    ("T", 5, 1, 2), ("sc", 4), ("T", 2, 1, 1), ("T", 2, 0, 2), ("T", 3, 1, 2), ("T", 0, 1, 3),
+    ("T", 0, 0, 3), ("T", 1, 1, 3), ("T", 4, 0, 2), ("T", 1, 0, 3), ("T", 6, 1, 2), ("T", 0, 1, 4),
+    ("T", 2, 0, 3), ("T", 4, 0, 3), ("T", 1, 1, 4), ("T", 2, 1, 2), ("T", 3, 0, 2), ("T", 1, 0, 4),
+    ("T", 0, 0, 4), ("T", 2, 0, 4), ("norm", 2), ("T", 2, 1, 3), ("T", 5, 0, 3), ("T", 3, 0, 3), ("sc", 5),
+    ("T", 6, 1, 3), ("T", 6, 0, 2), ("T", 4, 1, 3), ("T", 1, 1, 5), ("T", 2, 1, 4), ("T", 0, 0, 5),
+    ("T", 0, 1, 5), ("mix", 0), ("T", 1, 0, 5), ("T", 3, 1, 3), ("mix", 1), ("pool", 0), ("pool", 1),
+    ("pool", 2), ("T", 4, 0, 4), ("pool", 3), ("share", 3), ("share", 1), ("T", 4, 1, 4), ("T", 5, 1, 3),
+    ("share", 0), ("mid", 3), ("share", 2), ("mid", 1), ("T", 2, 0, 5), ("T", 3, 0, 4), ("mid", 0),
+    ("mid", 2), ("up", 1, 0), ("T", 3, 1, 4), ("T", 6, 1, 4), ("T", 4, 0, 5), ("T", 2, 1, 5),
+    ("T", 6, 0, 3), ("up", 1, 1), ("T", 4, 1, 5), ("dn", 4, 0), ("dn", 4, 1), ("dn", 4, 2), ("T", 5, 1, 4),
+    ("dn", 4, 3), ("T", 5, 0, 4), ("T", 3, 1, 5), ("up", 2, 1), ("T", 6, 0, 4), ("T", 3, 0, 5),
+    ("up", 2, 0), ("T", 5, 1, 5), ("T", 5, 0, 5), ("dn", 5, 1), ("dn", 5, 2), ("dn", 5, 3), ("dn", 5, 0),
+    ("T", 6, 0, 5), ("T", 6, 1, 5), ("last", 0), ("last", 1), ("own", 0), ("total", 0), ("total", 1),
+    ("own", 1), ("total", 2), ("total", 3), ("final", 0), ("final", 1), ("final", 2), ("final", 3),
 )
 ORDERS = (
-    ("xyz", "xzy"),
+    ("xzy", "xyz"),
+    ("xyz", "xyz"),
     ("xyz", "xyz"),
     ("xyz", "xzy"),
-    ("xyz", "xzy"),
-    ("xyz", "xzy"),
     ("xzy", "xzy"),
-    ("xyz", "zxy"),
+    ("xzy", "xzy"),
+    ("zxy", "xyz"),
 )
 
 
@@ -152,16 +152,16 @@
         return steps
 
     def start(self, key, src, dst, recv_sem, axis, at):
-        pool = self.unused.pop(0)
-        copy = send(src, dst, self.send_sem.at[pool], recv_sem, axis, at)
-        copy.start()
-        self.on_way.setdefault(key, []).append((pool, copy))
+        if key not in self.on_way:
+            self.on_way[key] = self.unused.pop(0)
+        send(src, dst, self.send_sem.at[self.on_way[key]], recv_sem, axis, at).start()
 
     def arrived(self, key, ref, recv_sem):
-        send(ref, ref, self.send_sem.at[0], recv_sem, "t", 1 - self.me["t"]).wait_recv()
-        for pool, copy in self.on_way.pop(key):
-            copy.wait_send()
-            self.unused.append(pool)
+        pool = self.on_way.pop(key)
+        copies = send(ref, ref, self.send_sem.at[pool], recv_sem, "t", 1 - self.me["t"])
+        copies.wait_recv()
+        copies.wait_send()
+        self.unused.append(pool)
 
     def tick(self, b, p, s):
         if s > 0:
@@ -267,29 +267,18 @@
     pairs = (
         (mix_in, mix_w),
         (group_in, group_w),
+        (up_in, up_w),
+        (down_in, down_w),
+        (gains_in, gains),
         (mix_s_in, mix_s),
         (group_s_in, group_s),
         (up_s_in, up_s),
         (down_s_in, down_s),
-        (up_in, up_w),
-        (down_in, down_w),
-        (gains_in, gains),
     )
     early = [load(k, src, dst) for k, (src, dst) in enumerate(pairs)]
     own_tokens = load(len(pairs), tokens, x_buf.at[t])
-    for copy in early[:6]:
-        copy.wait()
+    early[0].wait()
     w0[here[0], here[1], here[2], 0:64] = mix_w[...].astype(BF16)
-    w0[here[0], here[1], here[2], 64:80, 0:GW] = group_w[0].astype(BF16)
-    w0[here[0], here[1], here[2], 64:80, GW:] = group_w[1].astype(BF16)
-    scale_tile()
-    for copy in early[6:]:
-        copy.wait()
-    up_all, down_all = up_w[...].astype(BF16), down_w[...].astype(BF16)
-    for ref, lane in ((w1, 0), (w2, 1024)):
-        ref[here[0], here[1], here[2]] = up_all[:, lane : lane + 1024]
-    for ref, lane in ((w3, 0), (w4, 1024)):
-        ref[here[0], here[1], here[2]] = down_all[:, lane : lane + 1024]
     with jax.named_scope("greet"):
         greet(me, True)
 
@@ -302,6 +291,22 @@
     for p in range(2):
         gather.tick(0, p, 0)
     share(0, 0, tokens, x_buf.at[t])
+
+    for copy in early[5:]:
+        copy.wait()
+    scale_tile()
+    early[1].wait()
+    w0[here[0], here[1], here[2], 64:80, 0:GW] = group_w[0].astype(BF16)
+    w0[here[0], here[1], here[2], 64:80, GW:] = group_w[1].astype(BF16)
+    early[2].wait()
+    up_all = up_w[...].astype(BF16)
+    for ref, lane in ((w1, 0), (w2, 1024)):
+        ref[here[0], here[1], here[2]] = up_all[:, lane : lane + 1024]
+    early[3].wait()
+    down_all = down_w[...].astype(BF16)
+    for ref, lane in ((w3, 0), (w4, 1024)):
+        ref[here[0], here[1], here[2]] = down_all[:, lane : lane + 1024]
+    early[4].wait()
 
     def scales(step):
         if step == 0:
@@ -419,23 +424,16 @@
         weight = weight.reshape(512, width)
         cols = slice(512 * k, 512 * k + 512)
 
-        def body(i, _):
-            rows = pl.ds(pl.multiple_of(i * MROWS, MROWS), MROWS)
-            value = dot_t(hidden[rows, first : first + width], weight)
-            if buf > 3:
-                value = value + acc[half, rows, cols]
-            if b < NB - 1:
-                acc[half, rows, cols] = value
-            elif n < 2:
-                part_out[rows, cols] = value.astype(BF16)
-            else:
-                mixed[rows, cols] = value.astype(BF16)
-            return 0
-
-        if part is not None:
-            body(part, 0)
+        rows = ALL if part is None else pl.ds(part * MROWS, MROWS)
+        value = dot_t(hidden[rows, first : first + width], weight)
+        if buf > 3:
+            value = value + acc[half, rows, cols]
+        if b < NB - 1:
+            acc[half, rows, cols] = value
+        elif n < 2:
+            part_out[rows, cols] = value.astype(BF16)
         else:
-            lax.fori_loop(0, LENGTH // MROWS, body, 0)
+            mixed[rows, cols] = value.astype(BF16)
 
     def last(part):
         for n in range(2):

time: 102 us -> 99.7 us (0.977)
  Pallas kernels: 101 us -> 98.3 us
    pallas_call x1, Pallas kernels: 101 us -> 98.3 us  [on_device(): pl.pallas_call(kernel, out_shape=pltpu.VMEM((LENGTH, HALF), BF16), in_spe...]
where the time goes in v5:
time: 99.7 us; the launch traced here: 99.6 us
  Pallas kernels  98.3 us (99%)
  local copies, waits for them, and re-layouts  1.32 us (1%)
    pallas_call x1, Pallas kernels, on_device(): pl.pallas_call(kernel, out_shape=pltpu.VMEM((LENGTH, HALF), BF16), in_spe...  98.3 us

profile of v5, /device:TPU:1, one launch (start us, length us, event | category | flops | bytes accessed | tf_op | source)
XLA Modules:
  0.0 99.6 jit_solution(15947142209549166653)
XLA Ops:
  0.0 98.3 %shard_map.100 = bf16[1024,1024]{1,0:T(8,128)(2,1)S(1)} custom-call(bf16[1024,1024]{1,0:T(8,128)(2,1)} %tokens.1, f32[4,2048]{1,0:T(4,128)} %gains_in.1, f32[64,1024]{1,0:T(8,128)} %mix_in.1, f32[2,16,512]{2,1,0:T(8,128)} %group_in.1, f32[64,2048]{1,0:T(8,128)} %up_in.1, f32[64,2048]{1,0:T(8,128)} %bitcast.5, f32[2,16]{1,0:T(2,128)} %bitcast.6, ...), custom_call_target="tpu_custom_call" | custom-call | tf_op jit(solution)/shard_map/pallas_call | solution.py:512
  98.3 1.3 %copy.12 = bf16[1024,1024]{1,0:T(8,128)(2,1)} copy(bf16[1024,1024]{1,0:T(8,128)(2,1)S(1)} %shard_map.100) | data formatting | bytes 4194304

commit v6 on v5

--- a/solution.py
+++ b/solution.py
@@ -438,7 +438,8 @@
     def last(part):
         for n in range(2):
             down(NB - 1, n, part)
-        share(2, part, part_out.at[rows_of(part, 512)], part_in.at[rows_of(part, 512)])
+            place = (rows_of(part, 512), pl.ds(512 * n, 512))
+            share(2, 2 * part + n, part_out.at[place], part_in.at[place])
 
     def last_own(part):
         for n in range(2, 4):
@@ -446,7 +447,8 @@
 
     def total(i):
         if i % 2 == 0:
-            arrived(2, i // 2, part_in.at[rows_of(i // 2, 512)])
+            for n in range(2):
+                arrived(2, i + n, part_in.at[rows_of(i // 2, 512), pl.ds(512 * n, 512)])
 
         def body(k, _):
             rows = pl.ds(pl.multiple_of(i * BLOCK + k * SUB, SUB), SUB)

time: 99.7 us -> 99.4 us (level)
  no operation moved by 1% of the time
where the time goes in v6:
time: 99.4 us; the launch traced here: 99.3 us
  Pallas kernels  98 us (99%)
  local copies, waits for them, and re-layouts  1.32 us (1%)
    pallas_call x1, Pallas kernels, on_device(): pl.pallas_call(kernel, out_shape=pltpu.VMEM((LENGTH, HALF), BF16), in_spe...  98 us

profile of v6, /device:TPU:1, one launch (start us, length us, event | category | flops | bytes accessed | tf_op | source)
XLA Modules:
  0.0 99.3 jit_solution(4235028742589090017)
XLA Ops:
  0.0 98.0 %shard_map.100 = bf16[1024,1024]{1,0:T(8,128)(2,1)S(1)} custom-call(bf16[1024,1024]{1,0:T(8,128)(2,1)} %tokens.1, f32[4,2048]{1,0:T(4,128)} %gains_in.1, f32[64,1024]{1,0:T(8,128)} %mix_in.1, f32[2,16,512]{2,1,0:T(8,128)} %group_in.1, f32[64,2048]{1,0:T(8,128)} %up_in.1, f32[64,2048]{1,0:T(8,128)} %bitcast.5, f32[2,16]{1,0:T(2,128)} %bitcast.6, ...), custom_call_target="tpu_custom_call" | custom-call | tf_op jit(solution)/shard_map/pallas_call | solution.py:514
  98.0 1.3 %copy.12 = bf16[1024,1024]{1,0:T(8,128)(2,1)} copy(bf16[1024,1024]{1,0:T(8,128)(2,1)S(1)} %shard_map.100) | data formatting | bytes 4194304
